TPU v7x, 32 devices: a whole 2x2x4 slice. The times are simulated.
32 devices in a mesh: sp: 8 (over z, x), tp: 4 (over y, core).
Axes of the slice: x: 2, y: 2, z: 4, core: 2. Of those that a mesh axis runs over, the one named last changes fastest.
Arguments:
- resid: bfloat16 [1024, 2048], P('sp'), may hold values from -6 to 6
- norm_gain: float32 [2048], replicated, may hold values from 0.1 to 1.9
- cotangent: bfloat16 [1024, 2048], P('sp'), may hold values from -6 to 6
- route_ids: int32 [1024, 2], P('sp'), may hold values from 0 to 7, all different within a row; in each aligned block of 128 rows (0 to 127, 128 to 255, ...) at most 48 rows name the same one
- route_weight: float32 [1024, 2], P('sp'), may hold values from 0.25 to 2.25
- expert_gate: bfloat16 [8, 2048, 2048], P('sp', None, 'tp'), may hold values from -0.125 to 0.125
- expert_up: bfloat16 [8, 2048, 2048], P('sp', None, 'tp'), may hold values from -0.125 to 0.125
- expert_down: bfloat16 [8, 2048, 2048], P('sp', 'tp'), may hold values from -0.125 to 0.125
- out_proj: bfloat16 [2048, 4096], P('sp', 'tp'), may hold values from -0.09375 to 0.09375
- mixed: bfloat16 [1024, 4096], P('sp', 'tp'), may hold values from -6 to 6
- query: bfloat16 [1024, 2048], P('sp', 'tp'), may hold values from -6 to 6
- key: bfloat16 [1024, 2048], P('sp', 'tp'), may hold values from -1.5 to 1.5
- value: bfloat16 [1024, 4096], P('sp', 'tp'), may hold values from -6 to 6
- log_decay: float32 [1024, 2048], P('sp', 'tp'), may hold values from -1 to 0, as said below
- span_state: float32 [8, 16, 128, 256], P('sp', 'tp'), may hold values from -24 to 24
Outputs:
- grad_expert_gate: bfloat16 [8, 2048, 2048], P('sp', None, 'tp')
- grad_expert_up: bfloat16 [8, 2048, 2048], P('sp', None, 'tp')
- grad_expert_down: bfloat16 [8, 2048, 2048], P('sp', 'tp')
- grad_out_proj: float32 [2048, 4096], P('sp', 'tp')
- grad_query: bfloat16 [1024, 2048], P('sp', 'tp')
- grad_key: bfloat16 [1024, 2048], P('sp', 'tp')
- grad_value: bfloat16 [1024, 4096], P('sp', 'tp')
- grad_log_decay: float32 [1024, 2048], P('sp', 'tp')
Inputs may be any that keep to these rules, and one draw needn't show every extreme that they name: `route_ids`: A row names 2 different experts. Within each aligned block of 128 rows (the rows of one index of sp) no expert is named by more than 48 rows, and in every draw some expert is named by exactly 48 rows of some block. `log_decay`: every entry is zero or negative.
All inputs are finite; a program needn't handle non-finite values.
Results may differ from a plain program's by a relative error of at most 0.023.
Values may be sent and summed in bfloat16 or wider, within the bound.
A program may use at most 128 MiB of HBM per device.

v0:
```python
import jax
import jax.numpy as jnp
from jax import lax
from jax.experimental import pallas as pl
from jax.sharding import PartitionSpec as P

KEY_CHANNELS = 128
DV = 256
TOP = 2


epsilon = 1e-06
highest = lax.Precision.HIGHEST


SIDE = 64


def triangle(length, upper):
    rows = lax.broadcasted_iota(jnp.int32, (length, length), 0)
    cols = lax.broadcasted_iota(jnp.int32, (length, length), 1)
    return rows <= cols if upper else rows >= cols


def dot(a, b, ca, cb, precision=None):
    return lax.dot_general(
        a, b, (((ca,), (cb,)), ((), ())), preferred_element_type=jnp.float32, precision=precision
    )


def short(values):
    return values.astype(jnp.bfloat16)


def summary_kernel(resid_ref, proj_ref, query_ref, decay_ref, grad_ref, cum_ref, out_ref):
    length = query_ref.shape[0]
    grad = short(dot(resid_ref[...], proj_ref[...], 1, 0))
    grad_ref[...] = grad
    ones = triangle(length, False).astype(jnp.float32)
    cum = dot(ones, decay_ref[...], 1, 0, highest)
    cum_ref[...] = cum
    query = query_ref[...].astype(jnp.float32) * KEY_CHANNELS ** (-0.5)
    out_ref[0, :, 0:DV] = short(dot(short(query * jnp.exp(cum)), grad, 0, 0))
    fill = jnp.ones((length, 2 * SIDE), jnp.float32)
    total = jnp.exp(dot(decay_ref[...], fill, 0, 0, highest))
    upper = short(total).astype(jnp.float32)
    lanes = lax.broadcasted_iota(jnp.int32, total.shape, 1)
    out_ref[0, :, DV : DV + 2 * SIDE] = short(jnp.where(lanes < SIDE, upper, total - upper))


def gradient_kernel(
    exit_ref, grad_ref, query_ref, key_ref, value_ref, cum_ref, state_ref,
    out_query, out_key, out_value, out_log,
):
    length = query_ref.shape[0]
    exit_short = exit_ref[0]
    exit_cot = exit_short.astype(jnp.float32)
    query_scale = KEY_CHANNELS ** (-0.5)
    cum = cum_ref[...]
    last = cum[length - 1 : length, :]
    middle = cum[length // 2 - 1 : length // 2, :]
    query = query_ref[...].astype(jnp.float32) * query_scale
    key = key_ref[...].astype(jnp.float32)
    grad = grad_ref[...]
    value = value_ref[...]
    state = state_ref[0, 0]
    rise = jnp.exp(cum - middle)
    fall = jnp.exp(middle - cum)
    to_end = jnp.exp(last - cum)
    causal = triangle(length, False)
    query_part = short(query * rise)
    key_part = short(key * fall)
    scores = short(jnp.where(causal, dot(query_part, key_part, 1, 1), 0.0))
    grad_scores = short(jnp.where(causal, dot(grad, value, 1, 1), 0.0))
    grad_query = rise * dot(grad_scores, key_part, 1, 0)
    grad_query = grad_query + jnp.exp(cum) * dot(grad, short(state), 1, 1)
    from_exit = dot(value, exit_short, 1, 1)
    key_end = key * to_end
    grad_key = fall * dot(grad_scores, query_part, 0, 0) + to_end * from_exit
    grad_value = dot(scores, grad, 0, 0) + dot(short(key_end), exit_short, 1, 0)
    product = dot(jnp.ones((8, DV), jnp.float32), state * exit_cot, 1, 1, highest)[0:1, :]
    tail = jnp.exp(last) * product + jnp.sum(key_end * from_exit, axis=0, keepdims=True)
    ones = triangle(length, True).astype(jnp.float32)
    out_log[...] = dot(ones, query * grad_query - key * grad_key, 1, 0, highest) + tail
    out_query[...] = short(grad_query * query_scale)
    out_key[...] = short(grad_key)
    out_value[...] = short(grad_value)


def on_device(
    resid,
    norm_gain,
    cotangent,
    route_ids,
    route_weight,
    expert_gate,
    expert_up,
    expert_down,
    out_proj,
    mixed,
    query,
    key,
    value,
    log_decay,
    span_state,
):
    tokens_here = resid.shape[0]
    model_width = resid.shape[1]
    sp_count = lax.axis_size("sp")
    tp_count = lax.axis_size("tp")
    experts = sp_count * expert_gate.shape[0]
    capacity = 3 * tokens_here // experts
    resid_f = resid.astype(jnp.float32)
    inverse_rms = lax.rsqrt(jnp.mean(resid_f * resid_f, axis=1, keepdims=True) + epsilon)
    unit_rows = resid_f * inverse_rms
    normed = (unit_rows * norm_gain).astype(jnp.bfloat16)
    pair_expert = route_ids.reshape(-1)
    onehot = (pair_expert[:, None] == jnp.arange(experts, dtype=jnp.int32)[None, :]).astype(
        jnp.int32
    )
    slot_rank = jnp.sum((jnp.cumsum(onehot, axis=0) - onehot) * onehot, axis=1)
    slot_of = pair_expert * capacity + slot_rank
    slot_pairs = slot_of[None, :] == jnp.arange(experts * capacity, dtype=jnp.int32)[:, None]
    slot_tokens = jnp.any(slot_pairs.reshape(experts * capacity, tokens_here, TOP), axis=2).astype(
        jnp.bfloat16
    )
    slot_weight = jnp.sum(jnp.where(slot_pairs, route_weight.reshape(1, -1), 0.0), axis=1)
    column_share = model_width // tp_count
    offset = lax.axis_index("tp") * column_share
    rows_in = jnp.dot(
        slot_tokens,
        lax.dynamic_slice_in_dim(normed, offset, column_share, 1),
        preferred_element_type=jnp.float32,
    ).astype(jnp.bfloat16)
    rows_cot = (
        jnp.dot(
            slot_tokens,
            lax.dynamic_slice_in_dim(cotangent, offset, column_share, 1),
            preferred_element_type=jnp.float32,
        )
        * slot_weight[:, None]
    )
    arrived = tuple(
        lax.all_to_all(
            rows.reshape(experts, capacity, -1), "sp", split_axis=0, concat_axis=0, tiled=True
        ).reshape(1, experts * capacity, -1)
        for rows in (rows_in, rows_cot.astype(jnp.bfloat16))
    )
    mixed_all = lax.all_gather(mixed, "sp", axis=0, tiled=True)
    expert_in, expert_cot = (
        lax.all_gather(arrived[0], "tp", axis=2, tiled=True),
        lax.all_gather(arrived[1], "tp", axis=2, tiled=True),
    )
    gate_pre = jnp.einsum(
        "erd,edf->erf", expert_in, expert_gate, preferred_element_type=jnp.float32
    )
    up_pre = jnp.einsum("erd,edf->erf", expert_in, expert_up, preferred_element_type=jnp.float32)
    gate_sig = jax.nn.sigmoid(gate_pre)
    hidden = (gate_pre * gate_sig * up_pre).astype(jnp.bfloat16)
    grad_hidden = jnp.einsum(
        "erd,efd->erf", expert_cot, expert_down, preferred_element_type=jnp.float32
    )
    grad_up_act = (grad_hidden * gate_pre * gate_sig).astype(jnp.bfloat16)
    grad_gate_act = (grad_hidden * up_pre * gate_sig * (1.0 + gate_pre * (1.0 - gate_sig))).astype(
        jnp.bfloat16
    )
    grad_down_w = jnp.einsum("erf,erd->efd", hidden, expert_cot, preferred_element_type=jnp.float32)
    grad_gate_w = jnp.einsum(
        "erd,erf->edf", expert_in, grad_gate_act, preferred_element_type=jnp.float32
    )
    grad_up_w = jnp.einsum(
        "erd,erf->edf", expert_in, grad_up_act, preferred_element_type=jnp.float32
    )
    partial_value = jnp.einsum(
        "erf,edf->erd", grad_gate_act, expert_gate, preferred_element_type=jnp.float32
    )
    partial_value = partial_value + jnp.einsum(
        "erf,edf->erd", grad_up_act, expert_up, preferred_element_type=jnp.float32
    )
    partial_short = partial_value.astype(jnp.bfloat16)
    summed = (
        lax.psum_scatter(partial_short, "tp", scatter_dimension=2, tiled=True)
        .astype(jnp.float32)
        .astype(jnp.bfloat16)
    )
    returned = lax.all_to_all(
        summed.reshape(experts, capacity, -1), "sp", split_axis=0, concat_axis=0, tiled=True
    )
    flat_rows = returned.reshape(experts * capacity, -1)
    grad_normed = lax.all_gather(
        lax.dot_general(
            slot_tokens, flat_rows, (((0,), (0,)), ((), ())), preferred_element_type=jnp.float32
        ).astype(jnp.bfloat16),
        "tp",
        axis=1,
        tiled=True,
    ).astype(jnp.float32)
    scaled = grad_normed * norm_gain
    grad_resid = cotangent.astype(jnp.float32) + inverse_rms * (
        scaled - unit_rows * jnp.mean(scaled * unit_rows, axis=1, keepdims=True)
    )
    grad_resid = grad_resid.astype(jnp.bfloat16)
    resid_all = lax.all_to_all(grad_resid, "sp", split_axis=1, concat_axis=0, tiled=True)
    proj_all = lax.all_gather(out_proj, "sp", axis=0, tiled=True)
    heads = query.shape[1] // KEY_CHANNELS
    narrow = pl.BlockSpec((tokens_here, KEY_CHANNELS), lambda h: (0, h))
    wide = pl.BlockSpec((tokens_here, DV), lambda h: (0, h))
    packed = DV + 2 * SIDE
    grad_mixed, cum, own = pl.pallas_call(
        summary_kernel,
        grid=(heads,),
        in_specs=[
            pl.BlockSpec((tokens_here, model_width), lambda h: (0, 0)),
            pl.BlockSpec((model_width, DV), lambda h: (0, h)),
            narrow,
            narrow,
        ],
        out_specs=[wide, narrow, pl.BlockSpec((1, KEY_CHANNELS, packed), lambda h: (h, 0, 0))],
        out_shape=[
            jax.ShapeDtypeStruct((tokens_here, heads * DV), jnp.bfloat16),
            jax.ShapeDtypeStruct((tokens_here, heads * KEY_CHANNELS), jnp.float32),
            jax.ShapeDtypeStruct((heads, KEY_CHANNELS, packed), jnp.bfloat16),
        ],
        cost_estimate=pl.CostEstimate(
            flops=2 * tokens_here * heads * DV * (model_width + 2 * KEY_CHANNELS),
            bytes_accessed=2 * model_width * heads * DV + 8 * tokens_here * heads * DV,
            transcendentals=tokens_here * heads * KEY_CHANNELS,
        ),
        name="summary",
    )(grad_resid, proj_all, query, log_decay)
    share = KEY_CHANNELS // sp_count
    own_rows = own.reshape(heads, sp_count, share, packed).transpose(1, 0, 2, 3)
    spans = lax.all_to_all(
        own_rows.reshape(sp_count, heads * share, packed),
        "sp",
        split_axis=0,
        concat_axis=0,
        tiled=True,
    ).astype(jnp.float32)
    running = jnp.zeros((heads * share, DV), jnp.float32)
    exits = [running]
    for span in range(sp_count - 1, 0, -1):
        factor = spans[span, :, DV : DV + 1] + spans[span, :, DV + SIDE : DV + SIDE + 1]
        running = spans[span, :, :DV] + factor * running
        exits.append(running)
    exit_rows = lax.all_to_all(
        jnp.stack(exits[::-1]).astype(jnp.bfloat16),
        "sp",
        split_axis=0,
        concat_axis=0,
        tiled=True,
    )
    exit_all = (
        exit_rows.reshape(sp_count, heads, share, DV)
        .transpose(1, 0, 2, 3)
        .reshape(heads, KEY_CHANNELS, DV)
    )
    grad_query, grad_key, grad_value, grad_log_decay = pl.pallas_call(
        gradient_kernel,
        grid=(heads,),
        in_specs=[
            pl.BlockSpec((1, KEY_CHANNELS, DV), lambda h: (h, 0, 0)),
            wide,
            narrow,
            narrow,
            wide,
            narrow,
            pl.BlockSpec((1, 1, KEY_CHANNELS, DV), lambda h: (0, h, 0, 0)),
        ],
        out_specs=[narrow, narrow, wide, narrow],
        out_shape=[
            jax.ShapeDtypeStruct(query.shape, jnp.bfloat16),
            jax.ShapeDtypeStruct(key.shape, jnp.bfloat16),
            jax.ShapeDtypeStruct(value.shape, jnp.bfloat16),
            jax.ShapeDtypeStruct(log_decay.shape, jnp.float32),
        ],
        cost_estimate=pl.CostEstimate(
            flops=40 * tokens_here * heads * DV * KEY_CHANNELS,
            bytes_accessed=2 * heads * KEY_CHANNELS * DV + 24 * tokens_here * heads * DV,
            transcendentals=5 * tokens_here * heads * KEY_CHANNELS,
        ),
        name="gradients",
    )(exit_all, grad_mixed, query, key, value, cum, span_state)
    grad_out_proj = lax.dot_general(
        resid_all, mixed_all, (((0,), (0,)), ((), ())), preferred_element_type=jnp.float32
    )
    return (
        grad_gate_w.astype(jnp.bfloat16),
        grad_up_w.astype(jnp.bfloat16),
        grad_down_w.astype(jnp.bfloat16),
        grad_out_proj,
        grad_query,
        grad_key,
        grad_value,
        grad_log_decay,
    )


def solution(mesh):
    return jax.shard_map(
        on_device,
        mesh=mesh,
        in_specs=(
            P("sp", None),
            P(),
            P("sp", None),
            P("sp", None),
            P("sp", None),
            P("sp", None, "tp"),
            P("sp", None, "tp"),
            P("sp", "tp", None),
            P("sp", "tp"),
            P("sp", "tp"),
            P("sp", "tp"),
            P("sp", "tp"),
            P("sp", "tp"),
            P("sp", "tp"),
            P("sp", "tp", None, None),
        ),
        out_specs=(
            P("sp", None, "tp"),
            P("sp", None, "tp"),
            P("sp", "tp", None),
            P("sp", "tp"),
            P("sp", "tp"),
            P("sp", "tp"),
            P("sp", "tp"),
            P("sp", "tp"),
        ),
        check_vma=False,
    )
```

profile of v0, /device:TPU:0, one launch (start us, length us, event | category | flops | bytes accessed | tf_op | source)
XLA Modules:
  0.0 245.6 jit_solution(101586564451020720)
XLA Ops:
  14.0 19.2 %all_to_all.44 = bf16[8,48,512]{2,1,0:T(8,128)(2,1)} all-to-all(bf16[8,48,512]{2,1,0:T(8,128)(2,1)S(1)} %bitcast.83), channel_id=1, replica_groups=mesh['sp'=8,'tp'=4] {'sp'}, dimensions={0} | all-to-all | bytes 786432 | tf_op jit(solution)/shard_map/all_to_all | solution.py:144
  34.9 15.1 %all_to_all.45 = bf16[8,48,512]{2,1,0:T(8,128)(2,1)} all-to-all(bf16[8,48,512]{2,1,0:T(8,128)(2,1)S(1)} %bitcast.84), channel_id=1, replica_groups=mesh['sp'=8,'tp'=4] {'sp'}, dimensions={0} | all-to-all | bytes 786432 | tf_op jit(solution)/shard_map/all_to_all | solution.py:144
  51.8 2.5 %fusion.6 = f32[384,512]{1,0:T(8,128)S(1)} fusion(bf16[1,2048,512]{2,1,0:T(8,128)(2,1)S(1)} %copy-done, bf16[1,384,2048]{2,1,0:T(8,128)(2,1)} %all-gather.5.cloned.1.call-done), kind=kOutput, calls=%fused_computation.10 | convolution fusion | flops 805306368 | bytes 4456448 | tf_op jit(solution)/shard_map/erd,edf->erf/dot_general | solution.py:154
  54.3 1.9 fusion.9
  56.2 16.8 %all-gather.7.cloned.1.call-done = bf16[1,384,2048]{2,1,0:T(8,128)(2,1)} async-done(((bf16[1,384,512]{2,1,0:T(8,128)(2,1)}), bf16[1,384,2048]{2,1,0:T(8,128)(2,1)}) %all-gather.7.cloned.1.call-update) | async-done | bytes 1572880 | tf_op jit(solution)/shard_map/all_gather | solution.py:152
  73.0 3.4 %multiply_convert_fusion.1 = (bf16[384,512]{1,0:T(8,128)(2,1)S(1)}, bf16[384,512]{1,0:T(8,128)(2,1)S(1)}) fusion(f32[384,512]{1,0:T(8,128)S(1)} %fusion.6, f32[384,512]{1,0:T(8,128)} %fusion.9, bf16[1,512,2048]{2,1,0:T(8,128)(2,1)} %param.22, bf16[1,384,2048]{2,1,0:T(8,128)(2,1)} %all-gather.7.cloned.1.call-done), kind=kOutput, calls=%fused_computation.34 | convolution fusion | flops 807862272 | bytes 6029312 | tf_op jit(solution)/shard_map/erd,efd->erf/dot_general | solution.py:160
  78.3 2.2 fusion.3
  81.1 27.6 %reduce-scatter.2.cloned.1.call-done = bf16[1,384,512]{2,1,0:T(8,128)(2,1)} async-done(((bf16[1,384,2048]{2,1,0:T(8,128)(2,1)}), bf16[1,384,512]{2,1,0:T(8,128)(2,1)}) %reduce-scatter.2.cloned.1.call-update) | async-done | bytes 393232 | tf_op jit(solution)/shard_map/reduce_scatter | solution.py:182
  108.7 5.5 %all-to-all-start.2 = ((bf16[8,48,512]{2,1,0:T(8,128)(2,1)}), bf16[8,48,512]{2,1,0:T(8,128)(2,1)S(1)}, u32[]{:S(2)}, u32[]{:S(2)}) async-start(bf16[8,48,512]{2,1,0:T(8,128)(2,1)} %bitcast.86), calls=%async_computation.3 | async-start | bytes 786432 | tf_op jit(solution)/shard_map/all_to_all | solution.py:186
  114.8 20.6 %all-to-all-done.2 = bf16[8,48,512]{2,1,0:T(8,128)(2,1)S(1)} async-done(((bf16[8,48,512]{2,1,0:T(8,128)(2,1)}), bf16[8,48,512]{2,1,0:T(8,128)(2,1)S(1)}, u32[]{:S(2)}, u32[]{:S(2)}) %all-to-all-start.2) | async-done | bytes 393248 | tf_op jit(solution)/shard_map/all_to_all | solution.py:186
  136.5 6.5 %all_gather.17 = bf16[128,2048]{1,0:T(8,128)(2,1)S(1)} all-gather(bf16[128,512]{1,0:T(8,128)(2,1)S(1)} %convolution_convert_fusion.4), channel_id=1, replica_groups=mesh['sp'=8,'tp'=4] {'tp'}, dimensions={1}, use_global_device_ids=true | all-gather | bytes 655360 | tf_op jit(solution)/shard_map/all_gather | solution.py:190
  144.5 15.5 %all-gather.11.cloned.1.call-done.proj_ref = bf16[2048,1024]{1,0:T(8,128)(2,1)} async-done(((bf16[256,1024]{1,0:T(8,128)(2,1)}), bf16[2048,1024]{1,0:T(8,128)(2,1)}) %all-gather.11.cloned.1.call-update) | async-done | bytes 4194320 | tf_op jit(solution)/shard_map/all_gather | solution.py:204
  160.0 5.6 %summary.1 = (bf16[128,1024]{1,0:T(8,128)(2,1)}, f32[128,512]{1,0:T(8,128)}, bf16[4,128,384]{2,1,0:T(8,128)(2,1)}) custom-call(bf16[128,2048]{1,0:T(8,128)(2,1)} %add_convert_fusion.1.resid_ref, bf16[2048,1024]{1,0:T(8,128)(2,1)} %all-gather.11.cloned.1.call-done.proj_ref, bf16[128,512]{1,0:T(8,128)(2,1)} %query_ref.3, f32[128,512]{1,0:T(8,128)} %decay_ref.1), custom_call_target="tpu_custom_call" | custom-call | flops 603979776 | bytes 5242880 | tf_op jit(solution)/shard_map/summary/pallas_call | solution.py:209
  165.6 1.8 copy.56
  167.4 3.5 %all-to-all-start.4 = ((bf16[8,64,384]{2,1,0:T(8,128)(2,1)}), bf16[8,64,384]{2,1,0:T(8,128)(2,1)S(1)}, u32[]{:S(2)}, u32[]{:S(2)}) async-start(bf16[8,64,384]{2,1,0:T(8,128)(2,1)} %bitcast.21), calls=%async_computation.5 | async-start | bytes 786432 | tf_op jit(solution)/shard_map/all_to_all | solution.py:233
  171.0 4.2 %fusion.1 = bf16[1,2048,512]{2,1,0:T(8,128)(2,1)} fusion(bf16[384,512]{1,0:T(8,128)(2,1)S(1)} %copy-done.8, bf16[1,384,2048]{2,1,0:T(8,128)(2,1)} %all-gather.5.cloned.1.call-done), kind=kOutput, calls=%fused_computation.5 | convolution fusion | flops 806354944 | bytes 4063232 | tf_op jit(solution)/shard_map/erd,erf->edf/dot_general | solution.py:171
  175.2 2.7 %fusion.2 = bf16[1,512,2048]{2,1,0:T(8,128)(2,1)} fusion(bf16[1,384,2048]{2,1,0:T(8,128)(2,1)S(1)} %copy-done.15, f32[384,512]{1,0:T(8,128)S(1)} %copy-done.18, f32[384,512]{1,0:T(8,128)S(1)} %copy-done.17), kind=kOutput, calls=%fused_computation.6 | convolution fusion | flops 807534592 | bytes 5242880 | tf_op jit(solution)/shard_map/erf,erd->efd/dot_general | solution.py:167
  178.7 10.3 %all-to-all-done.4 = bf16[8,64,384]{2,1,0:T(8,128)(2,1)S(1)} async-done(((bf16[8,64,384]{2,1,0:T(8,128)(2,1)}), bf16[8,64,384]{2,1,0:T(8,128)(2,1)S(1)}, u32[]{:S(2)}, u32[]{:S(2)}) %all-to-all-start.4) | async-done | bytes 393248 | tf_op jit(solution)/shard_map/all_to_all | solution.py:233
  189.0 3.6 %all-to-all-start.3 = ((bf16[128,8,256]{2,0,1:T(8,128)(2,1)}), bf16[128,8,256]{2,0,1:T(8,128)(2,1)S(1)}, u32[]{:S(2)}, u32[]{:S(2)}) async-start(bf16[128,8,256]{2,0,1:T(8,128)(2,1)} %bitcast.77), calls=%async_computation.4 | async-start | bytes 1048576 | tf_op jit(solution)/shard_map/all_to_all | solution.py:203
  194.2 27.0 %all-to-all-done.3 = bf16[128,8,256]{2,0,1:T(8,128)(2,1)S(1)} async-done(((bf16[128,8,256]{2,0,1:T(8,128)(2,1)}), bf16[128,8,256]{2,0,1:T(8,128)(2,1)S(1)}, u32[]{:S(2)}, u32[]{:S(2)}) %all-to-all-start.3) | async-done | bytes 524320 | tf_op jit(solution)/shard_map/all_to_all | solution.py:203
  221.3 3.4 %all-to-all-start.5 = ((bf16[8,64,256]{2,1,0:T(8,128)(2,1)}), bf16[8,64,256]{2,1,0:T(8,128)(2,1)S(1)}, u32[]{:S(2)}, u32[]{:S(2)}) async-start(bf16[8,64,256]{2,1,0:T(8,128)(2,1)} %copy-done.11), calls=%async_computation.6 | async-start | bytes 524288 | tf_op jit(solution)/shard_map/all_to_all | solution.py:246
  224.7 4.0 %fusion = bf16[1,2048,512]{2,1,0:T(8,128)(2,1)} fusion(bf16[384,512]{1,0:T(8,128)(2,1)S(1)} %copy-done.10, bf16[1,384,2048]{2,1,0:T(8,128)(2,1)} %all-gather.5.cloned.1.call-done), kind=kOutput, calls=%fused_computation.4 | convolution fusion | flops 806354944 | bytes 4063232 | tf_op jit(solution)/shard_map/erd,erf->edf/dot_general | solution.py:168
  228.7 3.3 %fusion.45 = f32[256,1024]{1,0:T(8,128)} fusion(bf16[1024,256]{1,0:T(8,128)(2,1)S(1)} %bitcast.79, bf16[1024,1024]{1,0:T(8,128)(2,1)} %all-gather.9.cloned.1.call-done), kind=kOutput, calls=%fused_computation.93 | convolution fusion | flops 536870912 | bytes 3670016 | tf_op jit(solution)/shard_map/dot_general | solution.py:284
  233.9 4.6 %gradients.1 = (bf16[128,512]{1,0:T(8,128)(2,1)}, bf16[128,512]{1,0:T(8,128)(2,1)}, bf16[128,1024]{1,0:T(8,128)(2,1)}, f32[128,512]{1,0:T(8,128)}) custom-call(bf16[4,128,256]{2,1,0:T(8,128)(2,1)} %bitcast.88, bf16[128,1024]{1,0:T(8,128)(2,1)} %get-tuple-element.16.grad_ref, bf16[128,512]{1,0:T(8,128)(2,1)} %query_ref.3, bf16[128,512]{1,0:T(8,128)(2,1)} %key_ref.1, ...), custom_call_target="tpu_custom_call" | custom-call | flops 671088640 | bytes 3407872 | tf_op jit(solution)/shard_map/gradients/pallas_call | solution.py:258
  (91 shorter events, 19.2 us)
Async XLA Ops:
  8.0 43.8 %copy-start = (bf16[1,2048,512]{2,1,0:T(8,128)(2,1)S(1)}, bf16[1,2048,512]{2,1,0:T(8,128)(2,1)}, u32[]{:S(2)}) copy-start(bf16[1,2048,512]{2,1,0:T(8,128)(2,1)} %param.20) | copy-start | bytes 6291460
  8.0 5.6 %copy-start.12 = (f32[2048]{0:T(1024)S(1)}, f32[2048]{0:T(1024)}, u32[]{:S(2)}) copy-start(f32[2048]{0:T(1024)} %param.16) | copy-start | bytes 24580
  8.0 43.8 %all-gather.5.cloned.1.call-start = ((), (), s32[]{:S(2)}) async-start(), calls=%async_computation.7 | async-start | bytes 1966080 | tf_op jit(solution)/shard_map/all_gather | solution.py:151
  10.2 23.1 %copy-start.13 = (f32[128,2]{0,1:T(2,128)S(1)}, f32[128,2]{0,1:T(2,128)}, u32[]{:S(2)}) copy-start(f32[128,2]{0,1:T(2,128)} %param.19) | copy-start | bytes 3076
  11.2 23.7 %copy-start.6 = (pred[384,128]{1,0:T(8,128)(4,1)}, pred[384,128]{1,0:T(8,128)(4,1)S(1)}, u32[]{:S(2)}) copy-start(pred[384,128]{1,0:T(8,128)(4,1)S(1)} %fusion.22) | copy-start | bytes 147460
  33.3 39.7 %all-gather.7.cloned.1.call-start = ((), (), s32[]{:S(2)}) async-start(), calls=%async_computation.8 | async-start | bytes 1966080 | tf_op jit(solution)/shard_map/all_gather | solution.py:152
  50.0 58.6 %reduce-scatter.2.cloned.1.call-start = ((), (), s32[]{:S(2)}) async-start(), calls=%async_computation.9 | async-start | bytes 1966080 | tf_op jit(solution)/shard_map/reduce_scatter | solution.py:182
  51.8 2.5 %copy-start.3 = (bf16[1,2048,512]{2,1,0:T(8,128)(2,1)S(1)}, bf16[1,2048,512]{2,1,0:T(8,128)(2,1)}, u32[]{:S(2)}) copy-start(bf16[1,2048,512]{2,1,0:T(8,128)(2,1)} %param.21) | copy-start | bytes 6291460
  51.8 2.5 %copy-start.14 = (bf16[1,384,2048]{2,1,0:T(8,128)(2,1)S(1)}, bf16[1,384,2048]{2,1,0:T(8,128)(2,1)}, u32[]{:S(2)}) copy-start(bf16[1,384,2048]{2,1,0:T(8,128)(2,1)} %all-gather.5.cloned.1.call-done) | copy-start | bytes 4718596
  54.3 18.7 %copy-start.16 = (f32[384,512]{1,0:T(8,128)}, f32[384,512]{1,0:T(8,128)S(1)}, u32[]{:S(2)}) copy-start(f32[384,512]{1,0:T(8,128)S(1)} %fusion.6) | copy-start | bytes 2359300
  80.5 62.5 %copy-start.1 = (bf16[128,2048]{1,0:T(8,128)(2,1)S(1)}, bf16[128,2048]{1,0:T(8,128)(2,1)}, u32[]{:S(2)}) copy-start(bf16[128,2048]{1,0:T(8,128)(2,1)} %param.15) | copy-start | bytes 1572868
  80.5 62.8 %copy-start.5 = (bf16[128,2048]{1,0:T(8,128)(2,1)S(1)}, bf16[128,2048]{1,0:T(8,128)(2,1)}, u32[]{:S(2)}) copy-start(bf16[128,2048]{1,0:T(8,128)(2,1)} %param.17) | copy-start | bytes 1572868
  80.5 79.5 %all-gather.11.cloned.1.call-start = ((), (), s32[]{:S(2)}) async-start(), calls=%async_computation.11 | async-start | bytes 4718592 | tf_op jit(solution)/shard_map/all_gather | solution.py:204
  108.7 26.7 %all-to-all-start.2 = ((bf16[8,48,512]{2,1,0:T(8,128)(2,1)}), bf16[8,48,512]{2,1,0:T(8,128)(2,1)S(1)}, u32[]{:S(2)}, u32[]{:S(2)}) async-start(bf16[8,48,512]{2,1,0:T(8,128)(2,1)} %bitcast.86), calls=%async_computation.3 | async-start | bytes 786432 | tf_op jit(solution)/shard_map/all_to_all | solution.py:186
  114.2 114.5 %all-gather.9.cloned.1.call-start = ((), (), s32[]{:S(2)}) async-start(), calls=%async_computation.10 | async-start | bytes 2359296 | tf_op jit(solution)/shard_map/all_gather | solution.py:149
  144.5 26.4 %copy-start.8 = (bf16[384,512]{1,0:T(8,128)(2,1)S(1)}, bf16[384,512]{1,0:T(8,128)(2,1)}, u32[]{:S(2)}) copy-start(bf16[384,512]{1,0:T(8,128)(2,1)} %copy-done.7) | copy-start | bytes 1179652
  167.4 21.6 %all-to-all-start.4 = ((bf16[8,64,384]{2,1,0:T(8,128)(2,1)}), bf16[8,64,384]{2,1,0:T(8,128)(2,1)S(1)}, u32[]{:S(2)}, u32[]{:S(2)}) async-start(bf16[8,64,384]{2,1,0:T(8,128)(2,1)} %bitcast.21), calls=%async_computation.5 | async-start | bytes 786432 | tf_op jit(solution)/shard_map/all_to_all | solution.py:233
  170.9 4.2 %copy-start.15 = (bf16[1,384,2048]{2,1,0:T(8,128)(2,1)S(1)}, bf16[1,384,2048]{2,1,0:T(8,128)(2,1)}, u32[]{:S(2)}) copy-start(bf16[1,384,2048]{2,1,0:T(8,128)(2,1)} %all-gather.7.cloned.1.call-done) | copy-start | bytes 4718596
  170.9 4.2 %copy-start.17 = (f32[384,512]{1,0:T(8,128)S(1)}, f32[384,512]{1,0:T(8,128)}, u32[]{:S(2)}) copy-start(f32[384,512]{1,0:T(8,128)} %copy-done.16) | copy-start | bytes 2359300
  171.0 4.2 %copy-start.18 = (f32[384,512]{1,0:T(8,128)S(1)}, f32[384,512]{1,0:T(8,128)}, u32[]{:S(2)}) copy-start(f32[384,512]{1,0:T(8,128)} %fusion.9) | copy-start | bytes 2359300
  175.2 2.7 %copy-start.2 = (bf16[128,2048]{1,0:T(8,128)(2,1)S(1)}, bf16[128,2048]{1,0:T(8,128)(2,1)}, u32[]{:S(2)}) copy-start(bf16[128,2048]{1,0:T(8,128)(2,1)} %add_convert_fusion.1.resid_ref) | copy-start | bytes 1572868
  189.0 35.7 %copy-start.10 = (bf16[384,512]{1,0:T(8,128)(2,1)S(1)}, bf16[384,512]{1,0:T(8,128)(2,1)}, u32[]{:S(2)}) copy-start(bf16[384,512]{1,0:T(8,128)(2,1)} %copy-done.9) | copy-start | bytes 1179652
  189.0 32.3 %all-to-all-start.3 = ((bf16[128,8,256]{2,0,1:T(8,128)(2,1)}), bf16[128,8,256]{2,0,1:T(8,128)(2,1)S(1)}, u32[]{:S(2)}, u32[]{:S(2)}) async-start(bf16[128,8,256]{2,0,1:T(8,128)(2,1)} %bitcast.77), calls=%async_computation.4 | async-start | bytes 1048576 | tf_op jit(solution)/shard_map/all_to_all | solution.py:203
  221.3 11.9 %all-to-all-start.5 = ((bf16[8,64,256]{2,1,0:T(8,128)(2,1)}), bf16[8,64,256]{2,1,0:T(8,128)(2,1)S(1)}, u32[]{:S(2)}, u32[]{:S(2)}) async-start(bf16[8,64,256]{2,1,0:T(8,128)(2,1)} %copy-done.11), calls=%async_computation.6 | async-start | bytes 524288 | tf_op jit(solution)/shard_map/all_to_all | solution.py:246
  (4 other events, 4.7 us)
Sparse Core Ops, SparseCore 0:
  33.4 18.3 all-gather.4
  53.3 19.6 all-gather.6
  80.7 27.9 reduce-scatter.1
Sparse Core Ops, SparseCore 1:
  83.2 76.8 all-gather.10
  162.0 61.8 all-gather.8
where the time goes:
time: 247 us; the launch traced here: 246 us
  waiting for transfers between devices  122 us (49%)
  blocking collectives  40.8 us (17%)
  matrix products  27.6 us (11%)
  starting transfers between devices  16.3 us (7%)
  between operations  15.6 us (6%)
  Pallas kernels  10.2 us (4%)
  local copies, waits for them, and re-layouts  6.88 us (3%)
  other arithmetic  6.46 us (3%)
    all_to_all x2, blocking collectives, on_device(): lax.all_to_all(rows.reshape(experts, capacity, -1), 'sp', split_axis=0, c...  34.3 us
    reduce_scatter x1, waiting for transfers between devices, on_device(): lax.psum_scatter(partial_short, 'tp', scatter_dimension=2, tiled=True)  27.6 us
    all_to_all x1, waiting for transfers between devices, on_device(): lax.all_to_all(grad_resid, 'sp', split_axis=1, concat_axis=0, tiled=True)  27 us
    all_to_all x1, waiting for transfers between devices, on_device(): lax.all_to_all(summed.reshape(experts, capacity, -1), 'sp', split_axis=0,...  20.6 us
    all_gather x1, waiting for transfers between devices, on_device(): lax.all_gather(arrived[1], 'tp', axis=2, tiled=True)  16.8 us
    all_gather x1, waiting for transfers between devices, on_device(): proj_all = lax.all_gather(out_proj, 'sp', axis=0, tiled=True)  15.5 us
    all_to_all x1, waiting for transfers between devices, on_device(): lax.all_to_all(own_rows.reshape(sp_count, heads * share, packed), 'sp', s...  10.3 us
    all_gather x1, blocking collectives, on_device(): lax.all_gather(lax.dot_general(slot_tokens, flat_rows, (((0,), (0,)), (()...  6.5 us
  transfers between devices with their start and end apart: 9, of which 8 were waited for; matrix products, arithmetic and copies ran while one was open for 11% of the time, Pallas kernels for 2%

commit v1 on v0

v1 whole, which is shorter than its diff:
```python
import functools

import jax
import jax.numpy as jnp
from jax import lax
from jax.experimental import pallas as pl
from jax.experimental.pallas import tpu as pltpu
from jax.sharding import PartitionSpec as P

KEY_CHANNELS = 128
DV = 256
TOP = 2
CORES = 2
MESH = pl.DeviceIdType.MESH

epsilon = 1e-06
highest = lax.Precision.HIGHEST


def triangle(length, upper):
    rows = lax.broadcasted_iota(jnp.int32, (length, length), 0)
    cols = lax.broadcasted_iota(jnp.int32, (length, length), 1)
    return rows <= cols if upper else rows >= cols


def dot(a, b, ca, cb, precision=None):
    return lax.dot_general(
        a, b, (((ca,), (cb,)), ((), ())), preferred_element_type=jnp.float32, precision=precision
    )


def short(values):
    return values.astype(jnp.bfloat16)


def wide(values):
    return values.astype(jnp.float32)


def remote(src, dst, send, recv, device):
    return pltpu.make_async_remote_copy(
        src_ref=src, dst_ref=dst, send_sem=send, recv_sem=recv, device_id=device,
        device_id_type=MESH,
    )


def greet(sp, tp, n_sp, n_tp):
    barrier = pltpu.get_barrier_semaphore()
    for k in range(1, n_sp):
        pl.semaphore_signal(
            barrier, inc=1, device_id=(lax.rem(sp + k, n_sp), tp), device_id_type=MESH
        )
    for k in range(1, n_tp):
        pl.semaphore_signal(
            barrier, inc=1, device_id=(sp, lax.rem(tp + k, n_tp)), device_id_type=MESH
        )
    return barrier, n_sp + n_tp - 2


def expert_kernel(
    n_sp, n_tp, cap,
    ids_ref, weight_ref, resid_ref, cot_ref, gain_ref, gate_hbm, up_hbm, down_hbm,
    out_ref, ggate_hbm, gup_hbm, gdown_hbm,
    gate, up, down, ggate, gup, gdown,
    pick, sent, rows_in, gate_pre, up_pre, grad_hid, hidden, gact, uact,
    pair_sent, pair_got, own_sum, side_sent, side_got, final, back, gathered,
    load_sem, store_sem, out_s, out_r, side_s, side_r, twin_s, twin_r,
    pair_s, pair_r, red_s, red_r, ret_s, ret_r, gat_s, gat_r, gtw_s, gtw_r,
):
    sp, tp = lax.axis_index("sp"), lax.axis_index("tp")
    n_y = n_tp // CORES
    core, y = lax.rem(tp, CORES), lax.div(tp, CORES)
    twin = CORES * y + 1 - core
    tokens, model = resid_ref.shape
    cs = model // n_tp
    experts = n_sp
    rows = n_sp * cap
    fs = gate.shape[1]
    chunked = n_sp <= 8

    loads = [
        pltpu.make_async_copy(a, b, load_sem.at[i])
        for i, (a, b) in enumerate(((gate_hbm, gate), (up_hbm, up), (down_hbm, down)))
    ]
    for load in loads:
        load.start()
    barrier, others = greet(sp, tp, n_sp, n_tp)

    def at_y(j):
        return CORES * lax.rem(y + j, n_y) + core

    def from_y(j):
        return lax.rem(y - j + n_y, n_y)

    resid = wide(resid_ref[...])
    inverse = lax.rsqrt(jnp.mean(resid * resid, axis=1, keepdims=True) + epsilon)
    mine = pl.ds(pl.multiple_of(tp * cs, 128), cs)
    normed = short(wide(resid_ref[:, mine]) * inverse * gain_ref[:, mine])
    cot = cot_ref[:, mine]
    ids = ids_ref[...]
    weights = weight_ref[...]
    number = lax.broadcasted_iota(jnp.int32, (experts, tokens), 0)
    first, second = ids[0:1, :] == number, ids[1:2, :] == number
    member = jnp.logical_or(first, second)
    ahead = lax.broadcasted_iota(jnp.int32, (tokens, tokens), 0) < lax.broadcasted_iota(
        jnp.int32, (tokens, tokens), 1
    )
    rank = dot(
        jnp.where(member, 1.0, 0.0).astype(jnp.bfloat16),
        jnp.where(ahead, 1.0, 0.0).astype(jnp.bfloat16), 1, 0,
    )
    rank = jnp.where(member, rank, -1.0)
    weight = jnp.where(first, weights[0:1, :], 0.0) + jnp.where(second, weights[1:2, :], 0.0)
    places = lax.broadcasted_iota(jnp.int32, (cap, tokens), 0).astype(jnp.float32)
    for e in range(experts):
        chosen = places == rank[e : e + 1, :]
        one = jnp.where(chosen, 1.0, 0.0).astype(jnp.bfloat16)
        pick[e] = one
        scale = jnp.sum(jnp.where(chosen, weight[e : e + 1, :], 0.0), axis=1, keepdims=True)
        sent[e, 0] = short(dot(one, normed, 1, 0))
        sent[e, 1] = short(dot(one, cot, 1, 0) * scale)

    pl.semaphore_wait(barrier, others)

    def outgoing(k):
        d = lax.rem(sp + k, n_sp)
        return remote(sent.at[d], rows_in.at[tp, :, sp], out_s.at[k], out_r.at[k], (d, tp))

    def incoming(k):
        s = lax.rem(sp - k + n_sp, n_sp)
        return remote(sent.at[s], rows_in.at[tp, :, s], out_s.at[k], out_r.at[k], (s, tp))

    for k in range(1, n_sp):
        outgoing(k).start()
    rows_in[tp, :, sp] = sent[sp]

    pieces = n_sp if chunked else 1

    def piece(t, k):
        if not chunked:
            return rows_in.at[t]
        return rows_in.at[t, :, lax.rem(sp - k + n_sp, n_sp)]

    def to_side(j, k):
        return remote(
            piece(tp, k), piece(tp, k), side_s.at[j, k], side_r.at[j, k], (sp, at_y(j))
        )

    def from_side(j, k):
        t = CORES * from_y(j) + core
        return remote(piece(t, k), piece(t, k), side_s.at[j, k], side_r.at[j, k], (sp, t))

    def to_twin(j, k):
        t = CORES * from_y(j) + core
        return remote(piece(t, k), piece(t, k), twin_s.at[j, k], twin_r.at[j, k], (sp, twin))

    def from_twin(j, k):
        t = CORES * from_y(j) + 1 - core
        return remote(piece(t, k), piece(t, k), twin_s.at[j, k], twin_r.at[j, k], (sp, twin))

    if not chunked:
        for k in range(1, n_sp):
            incoming(k).wait_recv()
    for k in range(pieces):
        if chunked and k > 0:
            incoming(k).wait_recv()
        for j in range(1, n_y):
            to_side(j, k).start()
        to_twin(0, k).start()
    for k in range(pieces):
        for j in range(1, n_y):
            from_side(j, k).wait_recv()
            to_twin(j, k).start()
    for load in loads:
        load.wait()
    for k in range(pieces):
        for j in range(n_y):
            from_twin(j, k).wait_recv()

    gate_pre[...] = jnp.zeros_like(gate_pre)
    up_pre[...] = jnp.zeros_like(up_pre)
    grad_hid[...] = jnp.zeros_like(grad_hid)

    @pl.loop(0, n_tp)
    def _(p):
        part = pl.ds(pl.multiple_of(p * cs, 128), cs)
        block = rows_in[p, 0].reshape(rows, cs)
        gate_pre[...] += dot(block, gate[part, :], 1, 0)
        up_pre[...] += dot(block, up[part, :], 1, 0)
        grad_hid[...] += dot(rows_in[p, 1].reshape(rows, cs), down[:, part], 1, 1)

    @pl.loop(0, n_sp)
    def _(s):
        part = pl.ds(pl.multiple_of(s * cap, 16), cap)
        g, u, h = gate_pre[part, :], up_pre[part, :], grad_hid[part, :]
        sig = jax.nn.sigmoid(g)
        hidden[part, :] = short(g * sig * u)
        uact[part, :] = short(h * g * sig)
        gact[part, :] = short(h * u * sig * (1.0 + g * (1.0 - sig)))

    def partial(t):
        part = pl.ds(pl.multiple_of(t * cs, 128), cs)
        return dot(gact[...], gate[part, :], 1, 1) + dot(uact[...], up[part, :], 1, 1)

    def to_pair(j):
        return remote(pair_sent.at[j], pair_got.at[j], pair_s.at[j], pair_r.at[j], (sp, twin))

    for j in range(n_y):
        i = (j + 1) % n_y
        pair_sent[i] = short(partial(CORES * lax.rem(y + i, n_y) + 1 - core))
        to_pair(i).start()

    def span(k):
        return lax.rem(sp + k, n_sp)

    def to_red(j, k):
        dev = (sp, at_y(j))
        if not chunked:
            return remote(
                side_sent.at[j - 1], side_got.at[j - 1], red_s.at[j, k], red_r.at[j, k], dev
            )
        return remote(
            side_sent.at[j - 1, span(k)], side_got.at[j - 1, span(k)],
            red_s.at[j, k], red_r.at[j, k], dev,
        )

    order = list(range(1, n_sp)) + [0]
    for j in range(n_y):
        i = (j + 1) % n_y
        value = partial(at_y(i))
        to_pair(i).wait_recv()
        value = value + wide(pair_got[i])
        if i == 0:
            own_sum[...] = value.reshape(n_sp, cap, cs)
        else:
            side_sent[i - 1] = short(value).reshape(n_sp, cap, cs)
            for k in order if chunked else [0]:
                to_red(i, k).start()

    def unit(i):
        p = i % n_tp
        part = slice(p * cs, (p + 1) * cs)
        if i // n_tp == 0:
            ggate[part, :] = short(dot(rows_in[p, 0].reshape(rows, cs), gact[...], 0, 0))
        elif i // n_tp == 1:
            gup[part, :] = short(dot(rows_in[p, 0].reshape(rows, cs), uact[...], 0, 0))
        else:
            gdown[:, part] = short(dot(hidden[...], rows_in[p, 1].reshape(rows, cs), 0, 0))

    stores = [
        pltpu.make_async_copy(a, b, store_sem.at[i])
        for i, (a, b) in enumerate(((ggate, ggate_hbm), (gup, gup_hbm), (gdown, gdown_hbm)))
    ]
    units = 3 * n_tp
    done = 0

    def fill(upto):
        nonlocal done
        while done < min(upto, units):
            unit(done)
            done += 1
            if done % n_tp == 0:
                stores[done // n_tp - 1].start()

    def to_back(k):
        return remote(final.at[span(k)], back.at[sp], ret_s.at[k], ret_r.at[k], (span(k), tp))

    def from_back(k):
        s = lax.rem(sp - k + n_sp, n_sp)
        return remote(final.at[s], back.at[s], ret_s.at[k], ret_r.at[k], (s, tp))

    fill(n_tp // 2)
    for n, k in enumerate(order):
        total = own_sum[span(k)]
        for j in range(1, n_y):
            if chunked or n == 0:
                to_red(j, k if chunked else 0).wait_recv()
            total = total + wide(side_got[j - 1, span(k)])
        if k:
            final[span(k)] = short(total)
            to_back(k).start()
        else:
            back[sp] = short(total)
        if chunked:
            fill(done + 1)
    fill(units)

    for k in range(1, n_sp):
        from_back(k).wait_recv()
    gathered[tp] = short(
        dot(pick[...].reshape(rows, tokens), back[...].reshape(rows, cs), 0, 0)
    )

    def g_side(j):
        return remote(gathered.at[tp], gathered.at[tp], gat_s.at[j], gat_r.at[j], (sp, at_y(j)))

    def g_from_side(j):
        t = CORES * from_y(j) + core
        return remote(gathered.at[t], gathered.at[t], gat_s.at[j], gat_r.at[j], (sp, t))

    def g_twin(j):
        t = CORES * from_y(j) + core
        return remote(gathered.at[t], gathered.at[t], gtw_s.at[j], gtw_r.at[j], (sp, twin))

    def g_from_twin(j):
        t = CORES * from_y(j) + 1 - core
        return remote(gathered.at[t], gathered.at[t], gtw_s.at[j], gtw_r.at[j], (sp, twin))

    for j in range(1, n_y):
        g_side(j).start()
    g_twin(0).start()
    for j in range(1, n_y):
        g_from_side(j).wait_recv()
        g_twin(j).start()
    for j in range(n_y):
        g_from_twin(j).wait_recv()

    level = jnp.zeros((tokens, 1), jnp.float32)
    for p in range(n_tp):
        part = slice(p * cs, (p + 1) * cs)
        scaled = wide(gathered[p]) * gain_ref[:, part]
        level = level + jnp.sum(
            scaled * (wide(resid_ref[:, part]) * inverse), axis=1, keepdims=True
        )
    level = level * (1.0 / model)
    for p in range(n_tp):
        part = slice(p * cs, (p + 1) * cs)
        scaled = wide(gathered[p]) * gain_ref[:, part]
        unit_rows = wide(resid_ref[:, part]) * inverse
        out_ref[:, part] = short(
            wide(cot_ref[:, part]) + inverse * (scaled - unit_rows * level)
        )

    for k in range(1, n_sp):
        outgoing(k).wait_send()
        to_back(k).wait_send()
    for k in range(pieces):
        for j in range(1, n_y):
            to_side(j, k).wait_send()
            to_red(j, k).wait_send()
        for j in range(n_y):
            to_twin(j, k).wait_send()
    for j in range(n_y):
        to_pair(j).wait_send()
        g_twin(j).wait_send()
        if j:
            g_side(j).wait_send()
    for store in stores:
        store.wait()


def expert_call(n_sp, n_tp, ids, weights, resid, cot, gain, gate, up, down):
    tokens, model = resid.shape
    fs = gate.shape[1]
    cap = -(-(3 * tokens // n_sp) // 16) * 16
    cs = model // n_tp
    rows = n_sp * cap
    n_y = n_tp // CORES
    pieces = n_sp if n_sp <= 8 else 1
    bf, f32 = jnp.bfloat16, jnp.float32
    dma = pltpu.SemaphoreType.DMA
    side = max(1, n_y - 1)
    anywhere = pl.BlockSpec(memory_space=pl.ANY)
    local = pl.BlockSpec(memory_space=pltpu.VMEM)
    return pl.pallas_call(
        functools.partial(expert_kernel, n_sp, n_tp, cap),
        in_specs=[local] * 5 + [anywhere] * 3,
        out_specs=[local] + [anywhere] * 3,
        out_shape=[
            jax.ShapeDtypeStruct((tokens, model), bf),
            jax.ShapeDtypeStruct(gate.shape, bf),
            jax.ShapeDtypeStruct(up.shape, bf),
            jax.ShapeDtypeStruct(down.shape, bf),
        ],
        scratch_shapes=[
            pltpu.VMEM(gate.shape, bf), pltpu.VMEM(up.shape, bf), pltpu.VMEM(down.shape, bf),
            pltpu.VMEM(gate.shape, bf), pltpu.VMEM(up.shape, bf), pltpu.VMEM(down.shape, bf),
            pltpu.VMEM((n_sp, cap, tokens), bf),
            pltpu.VMEM((n_sp, 2, cap, cs), bf),
            pltpu.VMEM((n_tp, 2, n_sp, cap, cs), bf),
            pltpu.VMEM((rows, fs), f32), pltpu.VMEM((rows, fs), f32), pltpu.VMEM((rows, fs), f32),
            pltpu.VMEM((rows, fs), bf), pltpu.VMEM((rows, fs), bf), pltpu.VMEM((rows, fs), bf),
            pltpu.VMEM((n_y, rows, cs), bf), pltpu.VMEM((n_y, rows, cs), bf),
            pltpu.VMEM((n_sp, cap, cs), f32),
            pltpu.VMEM((side, n_sp, cap, cs), bf), pltpu.VMEM((side, n_sp, cap, cs), bf),
            pltpu.VMEM((n_sp, cap, cs), bf), pltpu.VMEM((n_sp, cap, cs), bf),
            pltpu.VMEM((n_tp, tokens, cs), bf),
            dma((3,)), dma((3,)),
            dma((n_sp,)), dma((n_sp,)),
            dma((n_y, pieces)), dma((n_y, pieces)), dma((n_y, pieces)), dma((n_y, pieces)),
            dma((n_y,)), dma((n_y,)),
            dma((n_y, pieces)), dma((n_y, pieces)),
            dma((n_sp,)), dma((n_sp,)),
            dma((n_y,)), dma((n_y,)), dma((n_y,)), dma((n_y,)),
        ],
        compiler_params=pltpu.CompilerParams(
            collective_id=0, has_side_effects=True, vmem_limit_bytes=52 * 2**20
        ),
        cost_estimate=pl.CostEstimate(
            flops=16 * rows * model * fs + 2 * 10**10, bytes_accessed=12 * model * fs,
            transcendentals=rows * fs,
        ),
        name="experts",
    )(ids, weights, resid, cot, gain, gate, up, down)


def attention_kernel(
    n_sp, n_tp, owners,
    resid_ref, proj_ref, mixed_ref, query_ref, key_ref, value_ref, decay_ref, state_ref,
    out_proj, out_query, out_key, out_value, out_log,
    grad, cum, own, totals, spans, decays, leave, exits, query_grad, key_part, resid_sent,
    resid_all,
    sum_s, sum_r, tot_s, tot_r, exit_s, exit_r, res_s, res_r,
):
    sp, tp = lax.axis_index("sp"), lax.axis_index("tp")
    tokens = query_ref.shape[0]
    heads = query_ref.shape[1] // KEY_CHANNELS
    share = heads * KEY_CHANNELS // owners
    features = resid_ref.shape[1] // n_sp
    scale = KEY_CHANNELS ** (-0.5)
    barrier, others = greet(sp, tp, n_sp, 1)
    lower = triangle(tokens, False)
    ones = lower.astype(jnp.float32)

    for d in range(n_sp):
        resid_sent[d] = resid_ref[:, d * features : (d + 1) * features]
    totals[...] = jnp.zeros_like(totals)
    for h in range(heads):
        narrow = slice(h * KEY_CHANNELS, (h + 1) * KEY_CHANNELS)
        broad = slice(h * DV, (h + 1) * DV)
        grad_h = short(dot(resid_ref[...], proj_ref[:, broad], 1, 0))
        grad[:, broad] = grad_h
        cum_h = dot(ones, decay_ref[:, narrow], 1, 0, highest)
        cum[:, narrow] = cum_h
        query = wide(query_ref[:, narrow]) * scale
        mine = short(dot(short(query * jnp.exp(cum_h)), grad_h, 0, 0))
        if share >= KEY_CHANNELS:
            own[h * KEY_CHANNELS // share, 0:KEY_CHANNELS] = mine
        else:
            each = KEY_CHANNELS // share
            own[h * each : (h + 1) * each] = mine.reshape(each, share, DV)
        totals[h : h + 1, :] = jnp.exp(cum_h[tokens - 1 : tokens, :])

    pl.semaphore_wait(barrier, others)

    def there(k):
        return lax.rem(sp + k, n_sp)

    def back(k):
        return lax.rem(sp - k + n_sp, n_sp)

    def when(test, action):
        if owners == n_sp:
            action()
        else:
            pl.when(test)(action)

    def to_sum(k):
        return remote(own.at[there(k)], spans.at[sp], sum_s.at[k], sum_r.at[k], (there(k), tp))

    def from_sum(k):
        return remote(spans.at[back(k)], spans.at[back(k)], sum_s.at[k], sum_r.at[k], (back(k), tp))

    def to_tot(k):
        return remote(totals, decays.at[sp], tot_s.at[k], tot_r.at[k], (there(k), tp))

    def from_tot(k):
        return remote(totals, decays.at[back(k)], tot_s.at[k], tot_r.at[k], (back(k), tp))

    def to_exit(k):
        return remote(leave.at[there(k)], exits.at[sp], exit_s.at[k], exit_r.at[k], (there(k), tp))

    def from_exit(k):
        return remote(exits.at[back(k)], exits.at[back(k)], exit_s.at[k], exit_r.at[k], (back(k), tp))

    def to_res(k):
        return remote(
            resid_sent.at[there(k)], resid_all.at[sp], res_s.at[k], res_r.at[k], (there(k), tp)
        )

    def from_res(k):
        return remote(
            resid_all.at[back(k)], resid_all.at[back(k)], res_s.at[k], res_r.at[k], (back(k), tp)
        )

    for k in range(1, n_sp):
        to_tot(k).start()
        when(there(k) < owners, lambda: to_sum(k).start())
    decays[sp] = totals[...]
    resid_all[sp] = resid_sent[sp]

    @functools.partial(when, sp < owners)
    def _():
        spans[sp] = own[sp]

    for h in range(heads):
        narrow = slice(h * KEY_CHANNELS, (h + 1) * KEY_CHANNELS)
        broad = slice(h * DV, (h + 1) * DV)
        cum_h = cum[:, narrow]
        middle = cum_h[tokens // 2 - 1 : tokens // 2, :]
        grad_h = grad[:, broad]
        query = wide(query_ref[:, narrow]) * scale
        key = wide(key_ref[:, narrow])
        rise, fall = jnp.exp(cum_h - middle), jnp.exp(middle - cum_h)
        query_part, key_near = short(query * rise), short(key * fall)
        scores = short(jnp.where(lower, dot(query_part, key_near, 1, 1), 0.0))
        grad_scores = short(
            jnp.where(lower, dot(grad_h, value_ref[:, broad], 1, 1), 0.0)
        )
        back_query = rise * dot(grad_scores, key_near, 1, 0)
        back_query = back_query + jnp.exp(cum_h) * dot(grad_h, short(state_ref[h]), 1, 1)
        query_grad[:, narrow] = query * back_query
        out_query[:, narrow] = short(back_query * scale)
        key_part[:, narrow] = fall * dot(grad_scores, query_part, 0, 0)
        out_value[:, broad] = short(dot(scores, grad_h, 0, 0))

    for k in range(1, n_sp):
        from_tot(k).wait_recv()
        when(sp < owners, lambda: from_sum(k).wait_recv())

    @functools.partial(when, sp < owners)
    def _():
        start = sp * share
        head = lax.div(start, KEY_CHANNELS)
        offset = lax.rem(start, KEY_CHANNELS)
        wanted = lax.broadcasted_iota(jnp.int32, (share, KEY_CHANNELS), 1) == offset + (
            lax.broadcasted_iota(jnp.int32, (share, KEY_CHANNELS), 0)
        )
        wanted = jnp.where(wanted, 1.0, 0.0)
        running = jnp.zeros((share, DV), jnp.float32)
        for s in range(n_sp - 1, -1, -1):
            leave[s] = short(running)
            if s:
                row = decays[s, pl.ds(head, 1), :]
                factor = jnp.sum(wanted * row, axis=1, keepdims=True)
                running = wide(spans[s]) + factor * running
        exits[sp] = leave[sp]

    for k in range(1, n_sp):
        when(sp < owners, lambda: to_exit(k).start())
    for k in range(1, n_sp):
        to_res(k).start()
    for k in range(1, n_sp):
        when(back(k) < owners, lambda: from_exit(k).wait_recv())

    upper = triangle(tokens, True).astype(jnp.float32)
    for h in range(heads):
        narrow = slice(h * KEY_CHANNELS, (h + 1) * KEY_CHANNELS)
        broad = slice(h * DV, (h + 1) * DV)
        each = KEY_CHANNELS // share
        exit_short = exits[h * each : (h + 1) * each].reshape(KEY_CHANNELS, DV)
        cum_h = cum[:, narrow]
        last = cum_h[tokens - 1 : tokens, :]
        key = wide(key_ref[:, narrow])
        to_end = jnp.exp(last - cum_h)
        from_end = dot(value_ref[:, broad], exit_short, 1, 1)
        key_end = key * to_end
        grad_key = key_part[:, narrow] + to_end * from_end
        product = dot(
            jnp.ones((8, DV), jnp.float32), state_ref[h] * wide(exit_short), 1, 1, highest
        )[0:1, :]
        tail = jnp.exp(last) * product + jnp.sum(key_end * from_end, axis=0, keepdims=True)
        out_log[:, narrow] = (
            dot(upper, query_grad[:, narrow] - key * grad_key, 1, 0, highest) + tail
        )
        out_key[:, narrow] = short(grad_key)
        out_value[:, broad] = short(
            wide(out_value[:, broad]) + dot(short(key_end), exit_short, 1, 0)
        )

    for k in range(1, n_sp):
        from_res(k).wait_recv()
    width = mixed_ref.shape[1]
    step = min(width, 256)
    for c in range(0, width, step):
        total = jnp.zeros((features, step), jnp.float32)
        for s in range(n_sp):
            total = total + dot(
                resid_all[s], mixed_ref[s * tokens : (s + 1) * tokens, c : c + step], 0, 0
            )
        out_proj[:, c : c + step] = total

    for k in range(1, n_sp):
        to_tot(k).wait_send()
        to_res(k).wait_send()
        when(there(k) < owners, lambda: to_sum(k).wait_send())
        when(sp < owners, lambda: to_exit(k).wait_send())


def attention_call(n_sp, n_tp, resid, proj, mixed, query, key, value, decay, state):
    tokens, model = resid.shape
    width = value.shape[1]
    heads = width // DV
    channels = heads * KEY_CHANNELS
    owners = min(n_sp, channels // 16)
    share = channels // owners
    features = model // n_sp
    bf, f32 = jnp.bfloat16, jnp.float32
    dma = pltpu.SemaphoreType.DMA
    local = pl.BlockSpec(memory_space=pltpu.VMEM)
    return pl.pallas_call(
        functools.partial(attention_kernel, n_sp, n_tp, owners),
        in_specs=[local] * 8,
        out_specs=[local] * 5,
        out_shape=[
            jax.ShapeDtypeStruct((features, width), f32),
            jax.ShapeDtypeStruct(query.shape, bf),
            jax.ShapeDtypeStruct(key.shape, bf),
            jax.ShapeDtypeStruct(value.shape, bf),
            jax.ShapeDtypeStruct(decay.shape, f32),
        ],
        scratch_shapes=[
            pltpu.VMEM((tokens, width), bf),
            pltpu.VMEM((tokens, channels), f32),
            pltpu.VMEM((owners, share, DV), bf),
            pltpu.VMEM((8 * -(-heads // 8), KEY_CHANNELS), f32),
            pltpu.VMEM((n_sp, share, DV), bf),
            pltpu.VMEM((n_sp, 8 * -(-heads // 8), KEY_CHANNELS), f32),
            pltpu.VMEM((n_sp, share, DV), bf),
            pltpu.VMEM((owners, share, DV), bf),
            pltpu.VMEM((tokens, channels), f32),
            pltpu.VMEM((tokens, channels), f32),
            pltpu.VMEM((n_sp, tokens, features), bf),
            pltpu.VMEM((n_sp, tokens, features), bf),
            *([dma((n_sp,))] * 8),
        ],
        compiler_params=pltpu.CompilerParams(
            collective_id=1, has_side_effects=True, vmem_limit_bytes=40 * 2**20
        ),
        cost_estimate=pl.CostEstimate(
            flops=10**10, bytes_accessed=2 * model * width, transcendentals=8 * tokens * channels
        ),
        name="attention",
    )(resid, proj, mixed, query, key, value, decay, state)


def on_device(
    resid,
    norm_gain,
    cotangent,
    route_ids,
    route_weight,
    expert_gate,
    expert_up,
    expert_down,
    out_proj,
    mixed,
    query,
    key,
    value,
    log_decay,
    span_state,
):
    n_sp = lax.axis_size("sp")
    n_tp = lax.axis_size("tp")
    proj_all = lax.all_gather(out_proj, "sp", axis=0, tiled=True)
    mixed_all = lax.all_gather(mixed, "sp", axis=0, tiled=True)
    grad_resid, grad_gate, grad_up, grad_down = expert_call(
        n_sp, n_tp, route_ids.T, route_weight.T, resid, cotangent, norm_gain.reshape(1, -1),
        expert_gate[0], expert_up[0], expert_down[0],
    )
    grad_proj, grad_query, grad_key, grad_value, grad_log = attention_call(
        n_sp, n_tp, grad_resid, proj_all, mixed_all, query, key, value, log_decay, span_state[0]
    )
    return (
        grad_gate[None],
        grad_up[None],
        grad_down[None],
        grad_proj,
        grad_query,
        grad_key,
        grad_value,
        grad_log,
    )


def solution(mesh):
    return jax.shard_map(
        on_device,
        mesh=mesh,
        in_specs=(
            P("sp", None),
            P(),
            P("sp", None),
            P("sp", None),
            P("sp", None),
            P("sp", None, "tp"),
            P("sp", None, "tp"),
            P("sp", "tp", None),
            P("sp", "tp"),
            P("sp", "tp"),
            P("sp", "tp"),
            P("sp", "tp"),
            P("sp", "tp"),
            P("sp", "tp"),
            P("sp", "tp", None, None),
        ),
        out_specs=(
            P("sp", None, "tp"),
            P("sp", None, "tp"),
            P("sp", "tp", None),
            P("sp", "tp"),
            P("sp", "tp"),
            P("sp", "tp"),
            P("sp", "tp"),
            P("sp", "tp"),
        ),
        check_vma=False,
    )
```

time: 247 us -> 200 us (0.81)
  Pallas kernels: 10.2 us -> 91.4 us
  waiting for transfers between devices: 122 us -> 75.8 us
  blocking collectives: 40.8 us -> 0 us
  matrix products: 27.6 us -> 0 us
  starting transfers between devices: 16.3 us -> 0.08 us
  local copies, waits for them, and re-layouts: 6.88 us -> 17.6 us
  other arithmetic: 6.46 us -> 0 us
    pallas_call x2, Pallas kernels: 10.2 us -> 91.4 us  [the longest x1 65.4 us: expert_call(): pl.pallas_call(functools.partial(expert_kernel, n_sp, n_tp, cap), in_spec...]
    all_to_all x4 -> x0, waiting for transfers between devices: 59.1 us -> none  [the longest x1 27 us: on_device(): lax.all_to_all(grad_resid, 'sp', split_axis=1, concat_axis=0, tiled=True)]
    all_gather x1, waiting for transfers between devices: 15.5 us -> 73.8 us  [on_device(): proj_all = lax.all_gather(out_proj, 'sp', axis=0, tiled=True)]
    all_to_all x2 -> x0, blocking collectives: 34.3 us -> none  [on_device(): lax.all_to_all(rows.reshape(experts, capacity, -1), 'sp', split_axis=0, c...]
    dot_general x12 -> x0, matrix products: 27.6 us -> none  [the longest x1 4.17 us: on_device(): jnp.einsum('erd,erf->edf', expert_in, grad_up_act, preferred_element_type...]
    reduce_scatter x1 -> x0, waiting for transfers between devices: 27.6 us -> none  [on_device(): lax.psum_scatter(partial_short, 'tp', scatter_dimension=2, tiled=True)]
    all_gather x2 -> x0, waiting for transfers between devices: 18.5 us -> none  [the longest x1 16.8 us: on_device(): lax.all_gather(arrived[1], 'tp', axis=2, tiled=True)]
    all_to_all x4 -> x0, starting transfers between devices: 16.1 us -> none  [the longest x1 5.51 us: on_device(): lax.all_to_all(summed.reshape(experts, capacity, -1), 'sp', split_axis=0,...]
  transfers between devices with their start and end apart: 9 -> 2, of which waited for: 8 -> 2; matrix products, arithmetic and copies ran while one was open for 11% -> 0% of each run, Pallas kernels for 2% -> 33%
where the time goes in v1:
time: 200 us; the launch traced here: 199 us
  Pallas kernels  91.4 us (46%)
  waiting for transfers between devices  75.8 us (38%)
  local copies, waits for them, and re-layouts  17.6 us (9%)
  between operations  14.1 us (7%)
    all_gather x1, waiting for transfers between devices, on_device(): proj_all = lax.all_gather(out_proj, 'sp', axis=0, tiled=True)  73.8 us
    pallas_call x1, Pallas kernels, expert_call(): pl.pallas_call(functools.partial(expert_kernel, n_sp, n_tp, cap), in_spec...  65.4 us
    pallas_call x1, Pallas kernels, attention_call(): pl.pallas_call(functools.partial(attention_kernel, n_sp, n_tp, owners), i...  26 us
    unnamed x38, local copies, waits for them, and re-layouts  17.6 us
  transfers between devices with their start and end apart: 2, of which 2 were waited for; matrix products, arithmetic and copies ran while one was open for 0% of the time, Pallas kernels for 33%

profile of v1, /device:TPU:0, one launch (start us, length us, event | category | flops | bytes accessed | tf_op | source)
XLA Modules:
  0.0 198.9 jit_solution(5627585093543441889)
XLA Ops:
  7.2 0.7 all-gather.5.cloned.1.call-update
  7.9 0.0 all-gather.3.cloned.1.call-start
  8.0 0.7 all-gather.3.cloned.1.call-update
  8.7 1.0 copy-done.2
  9.7 1.0 copy-done.3
  10.7 0.7 copy-done.9
  11.4 0.7 copy-done.10
  12.1 0.7 copy-done.11
  12.8 65.4 %experts.1 = (bf16[128,2048]{1,0:T(8,128)(2,1)S(1)}, bf16[2048,512]{1,0:T(8,128)(2,1)}, bf16[2048,512]{1,0:T(8,128)(2,1)}, bf16[512,2048]{1,0:T(8,128)(2,1)}) custom-call(s32[2,128]{1,0:T(2,128)S(1)} %bitcast.12, f32[2,128]{1,0:T(2,128)S(1)} %bitcast.13, bf16[128,2048]{1,0:T(8,128)(2,1)S(1)} %copy-done.2, bf16[128,2048]{1,0:T(8,128)(2,1)S(1)} %copy-done.3, ...), custom_call_target="tpu_custom_call" | custom-call | flops 26442450944 | bytes 12582912 | tf_op jit(solution)/shard_map/experts/pallas_call | solution.py:365
  78.2 0.6 all-gather.5.cloned.1.call-done.mixed_ref
  78.8 73.8 %all-gather.3.cloned.1.call-done.proj_ref = bf16[2048,1024]{1,0:T(8,128)(2,1)} async-done(((bf16[256,1024]{1,0:T(8,128)(2,1)}), bf16[2048,1024]{1,0:T(8,128)(2,1)}) %all-gather.3.cloned.1.call-update) | async-done | bytes 4194320 | tf_op jit(solution)/shard_map/all_gather | solution.py:656
  152.6 2.2 %copy-done = bf16[2048,1024]{1,0:T(8,128)(2,1)S(1)} copy-done((bf16[2048,1024]{1,0:T(8,128)(2,1)S(1)}, bf16[2048,1024]{1,0:T(8,128)(2,1)}, u32[]{:S(2)}) %copy-start) | copy-done | bytes 4194328
  154.8 1.6 copy-done.1
  156.4 26.0 %attention.1 = (f32[256,1024]{1,0:T(8,128)S(1)}, bf16[128,512]{1,0:T(8,128)(2,1)S(1)}, bf16[128,512]{1,0:T(8,128)(2,1)S(1)}, bf16[128,1024]{1,0:T(8,128)(2,1)S(1)}, f32[128,512]{1,0:T(8,128)S(1)}) custom-call(bf16[128,2048]{1,0:T(8,128)(2,1)S(1)} %get-tuple-element.20.resid_ref, bf16[2048,1024]{1,0:T(8,128)(2,1)S(1)} %copy-done, ...), custom_call_target="tpu_custom_call" | custom-call | flops 10000000000 | bytes 4194304 | tf_op jit(solution)/shard_map/attention/pallas_call | solution.py:601
  182.4 1.3 copy.31
  183.7 1.0 copy-done.13
  184.7 1.3 copy.32
  186.1 1.0 copy-done.12
  187.1 1.3 copy.33
  188.4 1.0 copy.34
  189.4 0.7 copy.35
  190.0 0.7 copy.36
  190.7 0.7 copy.37
  191.4 0.7 copy.38
  (22 shorter events, 0.1 us)
Async XLA Ops:
  7.2 71.6 %all-gather.5.cloned.1.call-start = ((), (), s32[]{:S(2)}) async-start(), calls=%async_computation.1 | async-start | bytes 2359296 | tf_op jit(solution)/shard_map/all_gather | solution.py:657
  7.9 144.7 %all-gather.3.cloned.1.call-start = ((), (), s32[]{:S(2)}) async-start(), calls=%async_computation | async-start | bytes 4718592 | tf_op jit(solution)/shard_map/all_gather | solution.py:656
  8.7 1.0 copy-start.2
  9.7 1.0 copy-start.3
  10.7 0.7 copy-start.9
  11.4 0.7 copy-start.10
  12.1 0.7 copy-start.11
  12.8 139.8 %copy-start.4 = (f32[1,4,128,256]{3,2,1,0:T(8,128)S(1)}, f32[1,4,128,256]{3,2,1,0:T(8,128)}, u32[]{:S(2)}) copy-start(f32[1,4,128,256]{3,2,1,0:T(8,128)} %param.29) | copy-start | bytes 1572868
  12.8 139.8 %copy-start.5 = (bf16[128,1024]{1,0:T(8,128)(2,1)S(1)}, bf16[128,1024]{1,0:T(8,128)(2,1)}, u32[]{:S(2)}) copy-start(bf16[128,1024]{1,0:T(8,128)(2,1)} %value_ref.1) | copy-start | bytes 786436
  12.8 139.8 %copy-start.6 = (f32[128,512]{1,0:T(8,128)S(1)}, f32[128,512]{1,0:T(8,128)}, u32[]{:S(2)}) copy-start(f32[128,512]{1,0:T(8,128)} %decay_ref.1) | copy-start | bytes 786436
  12.8 139.8 %copy-start.7 = (bf16[128,512]{1,0:T(8,128)(2,1)S(1)}, bf16[128,512]{1,0:T(8,128)(2,1)}, u32[]{:S(2)}) copy-start(bf16[128,512]{1,0:T(8,128)(2,1)} %query_ref.1) | copy-start | bytes 393220
  12.8 139.8 %copy-start.8 = (bf16[128,512]{1,0:T(8,128)(2,1)S(1)}, bf16[128,512]{1,0:T(8,128)(2,1)}, u32[]{:S(2)}) copy-start(bf16[128,512]{1,0:T(8,128)(2,1)} %key_ref.1) | copy-start | bytes 393220
  152.6 2.2 %copy-start = (bf16[2048,1024]{1,0:T(8,128)(2,1)S(1)}, bf16[2048,1024]{1,0:T(8,128)(2,1)}, u32[]{:S(2)}) copy-start(bf16[2048,1024]{1,0:T(8,128)(2,1)} %all-gather.3.cloned.1.call-done.proj_ref) | copy-start | bytes 12582916
  154.8 1.6 copy-start.1
  156.4 26.0 %copy-start.14 = (bf16[2048,512]{1,0:T(8,128)(2,1)S(1)}, bf16[2048,512]{1,0:T(8,128)(2,1)}, u32[]{:S(2)}) copy-start(bf16[2048,512]{1,0:T(8,128)(2,1)} %get-tuple-element.17) | copy-start | bytes 6291460
  182.4 2.3 %copy-start.13 = (bf16[2048,512]{1,0:T(8,128)(2,1)S(1)}, bf16[2048,512]{1,0:T(8,128)(2,1)}, u32[]{:S(2)}) copy-start(bf16[2048,512]{1,0:T(8,128)(2,1)} %get-tuple-element.18) | copy-start | bytes 6291460
  184.7 2.3 %copy-start.12 = (bf16[512,2048]{1,0:T(8,128)(2,1)S(1)}, bf16[512,2048]{1,0:T(8,128)(2,1)}, u32[]{:S(2)}) copy-start(bf16[512,2048]{1,0:T(8,128)(2,1)} %get-tuple-element.19) | copy-start | bytes 6291460
Sparse Core Ops, SparseCore 0:
  10.1 68.6 all-gather.4
  80.9 71.6 all-gather.2

commit v2 on v1

--- a/solution.py
+++ b/solution.py
@@ -1,4 +1,5 @@
 import functools
+import types
 
 import jax
 import jax.numpy as jnp
@@ -57,16 +58,149 @@
     return barrier, n_sp + n_tp - 2
 
 
-def expert_kernel(
-    n_sp, n_tp, cap,
-    ids_ref, weight_ref, resid_ref, cot_ref, gain_ref, gate_hbm, up_hbm, down_hbm,
-    out_ref, ggate_hbm, gup_hbm, gdown_hbm,
-    gate, up, down, ggate, gup, gdown,
-    pick, sent, rows_in, gate_pre, up_pre, grad_hid, hidden, gact, uact,
-    pair_sent, pair_got, own_sum, side_sent, side_got, final, back, gathered,
-    load_sem, store_sem, out_s, out_r, side_s, side_r, twin_s, twin_r,
-    pair_s, pair_r, red_s, red_r, ret_s, ret_r, gat_s, gat_r, gtw_s, gtw_r,
-):
+class Spread:
+    def __init__(self, n_sp, sp, tp, own, full, up_s, up_r, down_s, down_r, side_s, side_r):
+        self.own, self.full, self.tp = own, full, tp
+        self.sems = {1: (up_s, up_r), -1: (down_s, down_r), 0: (side_s, side_r)}
+        self.count = n_sp // 2
+        self.z, self.x = lax.div(sp, 2), lax.rem(sp, 2)
+
+    def exists(self, place):
+        return jnp.logical_and(place >= 0, place < self.count)
+
+    def sends(self, way, step):
+        return jnp.logical_and(
+            self.exists(self.z - way * (step - 1)), self.exists(self.z + way)
+        )
+
+    def along(self, way, step, half):
+        block = 2 * (self.z - way * (step - 1)) + self.x
+        src = self.own.at[half] if step == 1 else self.full.at[block, half]
+        send, recv = self.sems[way]
+        return remote(
+            src, self.full.at[block, half], send.at[step - 1, half], recv.at[step - 1, half],
+            (2 * (self.z + way) + self.x, self.tp),
+        )
+
+    def along_got(self, way, step, half):
+        block = 2 * (self.z - way * step) + self.x
+        there = self.full.at[block, half]
+        send, recv = self.sems[way]
+        return remote(
+            there, there, send.at[step - 1, half], recv.at[step - 1, half],
+            (2 * (self.z - way) + self.x, self.tp),
+        )
+
+    def across(self, way, step, half, got=False):
+        side = 1 - self.x if got else self.x
+        block = 2 * (self.z - way * step) + side
+        there = self.full.at[block, half]
+        src = self.own.at[half] if step == 0 and not got else there
+        send, recv = self.sems[0]
+        index = step if way == 1 else self.count - 1 + step
+        return remote(
+            src, there, send.at[index, half], recv.at[index, half],
+            (2 * self.z + 1 - self.x, self.tp),
+        )
+
+    def start(self):
+        for half in range(2):
+            for way in (1, -1):
+                pl.when(self.sends(way, 1))(lambda: self.along(way, 1, half).start())
+            self.across(1, 0, half).start()
+
+    def pump(self, step):
+        for half in range(2):
+            for way in (1, -1):
+                @pl.when(self.exists(self.z - way * step))
+                def _():
+                    self.along_got(way, step, half).wait_recv()
+                    if step < self.count - 1:
+                        pl.when(self.exists(self.z + way))(
+                            lambda: self.along(way, step + 1, half).start()
+                        )
+                    self.across(way, step, half).start()
+
+    def finish(self):
+        for half in range(2):
+            self.across(1, 0, half, True).wait_recv()
+            for step in range(1, self.count):
+                for way in (1, -1):
+                    pl.when(self.exists(self.z - way * step))(
+                        lambda: self.across(way, step, half, True).wait_recv()
+                    )
+
+    def drain(self):
+        for half in range(2):
+            self.across(1, 0, half).wait_send()
+            for step in range(1, self.count):
+                for way in (1, -1):
+                    pl.when(self.sends(way, step))(
+                        lambda: self.along(way, step, half).wait_send()
+                    )
+                    pl.when(self.exists(self.z - way * step))(
+                        lambda: self.across(way, step, half).wait_send()
+                    )
+
+
+def expert_phase(n_sp, n_tp, cap, projs, later, refs):
+    ids_hbm = refs.ids_hbm
+    weight_hbm = refs.weight_hbm
+    resid_hbm = refs.resid_hbm
+    cot_hbm = refs.cot_hbm
+    gain_hbm = refs.gain_hbm
+    gate_hbm = refs.gate_hbm
+    up_hbm = refs.up_hbm
+    down_hbm = refs.down_hbm
+    proj_hbm = refs.proj_hbm
+    ggate = refs.ggate
+    gup = refs.gup
+    gdown = refs.gdown
+    proj_all = refs.proj_all
+    ids_ref = refs.ids_ref
+    weight_ref = refs.weight_ref
+    resid_ref = refs.resid_ref
+    cot_ref = refs.cot_ref
+    gain_ref = refs.gain_ref
+    proj = refs.proj
+    gate = refs.gate
+    up = refs.up
+    down = refs.down
+    pick = refs.pick
+    sent = refs.sent
+    rows_in = refs.rows_in
+    gate_pre = refs.gate_pre
+    up_pre = refs.up_pre
+    grad_hid = refs.grad_hid
+    hidden = refs.hidden
+    gact = refs.gact
+    uact = refs.uact
+    pair_sent = refs.pair_sent
+    pair_got = refs.pair_got
+    own_sum = refs.own_sum
+    side_sent = refs.side_sent
+    side_got = refs.side_got
+    final = refs.final
+    back = refs.back
+    gathered = refs.gathered
+    load_sem = refs.load_sem
+    out_s = refs.out_s
+    out_r = refs.out_r
+    side_s = refs.side_s
+    side_r = refs.side_r
+    twin_s = refs.twin_s
+    twin_r = refs.twin_r
+    pair_s = refs.pair_s
+    pair_r = refs.pair_r
+    red_s = refs.red_s
+    red_r = refs.red_r
+    ret_s = refs.ret_s
+    ret_r = refs.ret_r
+    gat_s = refs.gat_s
+    gat_r = refs.gat_r
+    gtw_s = refs.gtw_s
+    gtw_r = refs.gtw_r
+    grad_resid = refs.grad_resid
     sp, tp = lax.axis_index("sp"), lax.axis_index("tp")
     n_y = n_tp // CORES
     core, y = lax.rem(tp, CORES), lax.div(tp, CORES)
@@ -80,11 +214,19 @@
 
     loads = [
         pltpu.make_async_copy(a, b, load_sem.at[i])
-        for i, (a, b) in enumerate(((gate_hbm, gate), (up_hbm, up), (down_hbm, down)))
+        for i, (a, b) in enumerate(
+            (
+                (resid_hbm, resid_ref), (cot_hbm, cot_ref), (ids_hbm, ids_ref),
+                (weight_hbm, weight_ref), (gain_hbm, gain_ref), (proj_hbm, proj),
+                (gate_hbm, gate), (up_hbm, up), (down_hbm, down),
+            )
+        )
     ]
     for load in loads:
         load.start()
     barrier, others = greet(sp, tp, n_sp, n_tp)
+    for load in loads[:5]:
+        load.wait()
 
     def at_y(j):
         return CORES * lax.rem(y + j, n_y) + core
@@ -120,6 +262,8 @@
         sent[e, 0] = short(dot(one, normed, 1, 0))
         sent[e, 1] = short(dot(one, cot, 1, 0) * scale)
 
+    for load in later:
+        load.start()
     pl.semaphore_wait(barrier, others)
 
     def outgoing(k):
@@ -132,6 +276,9 @@
 
     for k in range(1, n_sp):
         outgoing(k).start()
+    loads[5].wait()
+    projs.start()
+    proj_all[sp] = proj[...]
     rows_in[tp, :, sp] = sent[sp]
 
     pieces = n_sp if chunked else 1
@@ -171,11 +318,12 @@
         for j in range(1, n_y):
             from_side(j, k).wait_recv()
             to_twin(j, k).start()
-    for load in loads:
+    for load in loads[6:]:
         load.wait()
     for k in range(pieces):
         for j in range(n_y):
             from_twin(j, k).wait_recv()
+    projs.pump(1)
 
     gate_pre[...] = jnp.zeros_like(gate_pre)
     up_pre[...] = jnp.zeros_like(up_pre)
@@ -247,10 +395,6 @@
         else:
             gdown[:, part] = short(dot(hidden[...], rows_in[p, 1].reshape(rows, cs), 0, 0))
 
-    stores = [
-        pltpu.make_async_copy(a, b, store_sem.at[i])
-        for i, (a, b) in enumerate(((ggate, ggate_hbm), (gup, gup_hbm), (gdown, gdown_hbm)))
-    ]
     units = 3 * n_tp
     done = 0
 
@@ -259,8 +403,6 @@
         while done < min(upto, units):
             unit(done)
             done += 1
-            if done % n_tp == 0:
-                stores[done // n_tp - 1].start()
 
     def to_back(k):
         return remote(final.at[span(k)], back.at[sp], ret_s.at[k], ret_r.at[k], (span(k), tp))
@@ -284,6 +426,7 @@
         if chunked:
             fill(done + 1)
     fill(units)
+    projs.pump(2)
 
     for k in range(1, n_sp):
         from_back(k).wait_recv()
@@ -327,108 +470,95 @@
         part = slice(p * cs, (p + 1) * cs)
         scaled = wide(gathered[p]) * gain_ref[:, part]
         unit_rows = wide(resid_ref[:, part]) * inverse
-        out_ref[:, part] = short(
+        grad_resid[:, part] = short(
             wide(cot_ref[:, part]) + inverse * (scaled - unit_rows * level)
         )
 
-    for k in range(1, n_sp):
-        outgoing(k).wait_send()
-        to_back(k).wait_send()
-    for k in range(pieces):
-        for j in range(1, n_y):
-            to_side(j, k).wait_send()
-            to_red(j, k).wait_send()
+    for step in range(3, n_sp // 2):
+        projs.pump(step)
+
+    def drain():
+        for k in range(1, n_sp):
+            outgoing(k).wait_send()
+            to_back(k).wait_send()
+        for k in range(pieces):
+            for j in range(1, n_y):
+                to_side(j, k).wait_send()
+                to_red(j, k).wait_send()
+            for j in range(n_y):
+                to_twin(j, k).wait_send()
         for j in range(n_y):
-            to_twin(j, k).wait_send()
-    for j in range(n_y):
-        to_pair(j).wait_send()
-        g_twin(j).wait_send()
-        if j:
-            g_side(j).wait_send()
-    for store in stores:
-        store.wait()
-
-
-def expert_call(n_sp, n_tp, ids, weights, resid, cot, gain, gate, up, down):
-    tokens, model = resid.shape
-    fs = gate.shape[1]
-    cap = -(-(3 * tokens // n_sp) // 16) * 16
-    cs = model // n_tp
-    rows = n_sp * cap
-    n_y = n_tp // CORES
-    pieces = n_sp if n_sp <= 8 else 1
-    bf, f32 = jnp.bfloat16, jnp.float32
-    dma = pltpu.SemaphoreType.DMA
-    side = max(1, n_y - 1)
-    anywhere = pl.BlockSpec(memory_space=pl.ANY)
-    local = pl.BlockSpec(memory_space=pltpu.VMEM)
-    return pl.pallas_call(
-        functools.partial(expert_kernel, n_sp, n_tp, cap),
-        in_specs=[local] * 5 + [anywhere] * 3,
-        out_specs=[local] + [anywhere] * 3,
-        out_shape=[
-            jax.ShapeDtypeStruct((tokens, model), bf),
-            jax.ShapeDtypeStruct(gate.shape, bf),
-            jax.ShapeDtypeStruct(up.shape, bf),
-            jax.ShapeDtypeStruct(down.shape, bf),
-        ],
-        scratch_shapes=[
-            pltpu.VMEM(gate.shape, bf), pltpu.VMEM(up.shape, bf), pltpu.VMEM(down.shape, bf),
-            pltpu.VMEM(gate.shape, bf), pltpu.VMEM(up.shape, bf), pltpu.VMEM(down.shape, bf),
-            pltpu.VMEM((n_sp, cap, tokens), bf),
-            pltpu.VMEM((n_sp, 2, cap, cs), bf),
-            pltpu.VMEM((n_tp, 2, n_sp, cap, cs), bf),
-            pltpu.VMEM((rows, fs), f32), pltpu.VMEM((rows, fs), f32), pltpu.VMEM((rows, fs), f32),
-            pltpu.VMEM((rows, fs), bf), pltpu.VMEM((rows, fs), bf), pltpu.VMEM((rows, fs), bf),
-            pltpu.VMEM((n_y, rows, cs), bf), pltpu.VMEM((n_y, rows, cs), bf),
-            pltpu.VMEM((n_sp, cap, cs), f32),
-            pltpu.VMEM((side, n_sp, cap, cs), bf), pltpu.VMEM((side, n_sp, cap, cs), bf),
-            pltpu.VMEM((n_sp, cap, cs), bf), pltpu.VMEM((n_sp, cap, cs), bf),
-            pltpu.VMEM((n_tp, tokens, cs), bf),
-            dma((3,)), dma((3,)),
-            dma((n_sp,)), dma((n_sp,)),
-            dma((n_y, pieces)), dma((n_y, pieces)), dma((n_y, pieces)), dma((n_y, pieces)),
-            dma((n_y,)), dma((n_y,)),
-            dma((n_y, pieces)), dma((n_y, pieces)),
-            dma((n_sp,)), dma((n_sp,)),
-            dma((n_y,)), dma((n_y,)), dma((n_y,)), dma((n_y,)),
-        ],
-        compiler_params=pltpu.CompilerParams(
-            collective_id=0, has_side_effects=True, vmem_limit_bytes=52 * 2**20
-        ),
-        cost_estimate=pl.CostEstimate(
-            flops=16 * rows * model * fs + 2 * 10**10, bytes_accessed=12 * model * fs,
-            transcendentals=rows * fs,
-        ),
-        name="experts",
-    )(ids, weights, resid, cot, gain, gate, up, down)
-
-
-def attention_kernel(
-    n_sp, n_tp, owners,
-    resid_ref, proj_ref, mixed_ref, query_ref, key_ref, value_ref, decay_ref, state_ref,
-    out_proj, out_query, out_key, out_value, out_log,
-    grad, cum, own, totals, spans, decays, leave, exits, query_grad, key_part, resid_sent,
-    resid_all,
-    sum_s, sum_r, tot_s, tot_r, exit_s, exit_r, res_s, res_r,
-):
+            to_pair(j).wait_send()
+            g_twin(j).wait_send()
+            if j:
+                g_side(j).wait_send()
+
+    return drain
+
+
+def attention_phase(n_sp, n_tp, owners, mixeds, loads, refs):
+    query_hbm = refs.query_hbm
+    key_hbm = refs.key_hbm
+    value_hbm = refs.value_hbm
+    decay_hbm = refs.decay_hbm
+    state_hbm = refs.state_hbm
+    out_proj = refs.out_proj
+    out_query = refs.out_query
+    out_key = refs.out_key
+    out_value = refs.out_value
+    out_log = refs.out_log
+    mixed_all = refs.mixed_all
+    query_ref = refs.query_ref
+    key_ref = refs.key_ref
+    value_ref = refs.value_ref
+    decay_ref = refs.decay_ref
+    state_ref = refs.state_ref
+    grad = refs.grad
+    cum = refs.cum
+    own = refs.own
+    totals = refs.totals
+    spans = refs.spans
+    decays = refs.decays
+    leave = refs.leave
+    exits = refs.exits
+    query_grad = refs.query_grad
+    key_part = refs.key_part
+    resid_sent = refs.resid_sent
+    resid_all = refs.resid_all
+    sum_s = refs.sum_s
+    sum_r = refs.sum_r
+    tot_s = refs.tot_s
+    tot_r = refs.tot_r
+    exit_s = refs.exit_s
+    exit_r = refs.exit_r
+    res_s = refs.res_s
+    res_r = refs.res_r
+    more_sem = refs.more_sem
+    proj_all = refs.proj_all
+    grad_resid = refs.grad_resid
+    mixed = refs.mixed
+    mixed_hbm = refs.mixed_hbm
     sp, tp = lax.axis_index("sp"), lax.axis_index("tp")
     tokens = query_ref.shape[0]
     heads = query_ref.shape[1] // KEY_CHANNELS
     share = heads * KEY_CHANNELS // owners
-    features = resid_ref.shape[1] // n_sp
+    features = grad_resid.shape[1] // n_sp
     scale = KEY_CHANNELS ** (-0.5)
-    barrier, others = greet(sp, tp, n_sp, 1)
     lower = triangle(tokens, False)
     ones = lower.astype(jnp.float32)
 
     for d in range(n_sp):
-        resid_sent[d] = resid_ref[:, d * features : (d + 1) * features]
+        resid_sent[d] = grad_resid[:, d * features : (d + 1) * features]
     totals[...] = jnp.zeros_like(totals)
+    for load in loads:
+        load.wait()
+    mixeds.start()
+    mixed_all[sp] = mixed[...]
     for h in range(heads):
         narrow = slice(h * KEY_CHANNELS, (h + 1) * KEY_CHANNELS)
         broad = slice(h * DV, (h + 1) * DV)
-        grad_h = short(dot(resid_ref[...], proj_ref[:, broad], 1, 0))
+        proj_h = proj_all[:, :, :, broad].reshape(grad_resid.shape[1], DV)
+        grad_h = short(dot(grad_resid[...], proj_h, 1, 0))
         grad[:, broad] = grad_h
         cum_h = dot(ones, decay_ref[:, narrow], 1, 0, highest)
         cum[:, narrow] = cum_h
@@ -440,8 +570,6 @@
             each = KEY_CHANNELS // share
             own[h * each : (h + 1) * each] = mine.reshape(each, share, DV)
         totals[h : h + 1, :] = jnp.exp(cum_h[tokens - 1 : tokens, :])
-
-    pl.semaphore_wait(barrier, others)
 
     def there(k):
         return lax.rem(sp + k, n_sp)
@@ -514,6 +642,7 @@
         key_part[:, narrow] = fall * dot(grad_scores, query_part, 0, 0)
         out_value[:, broad] = short(dot(scores, grad_h, 0, 0))
 
+    mixeds.pump(1)
     for k in range(1, n_sp):
         from_tot(k).wait_recv()
         when(sp < owners, lambda: from_sum(k).wait_recv())
@@ -540,6 +669,7 @@
         when(sp < owners, lambda: to_exit(k).start())
     for k in range(1, n_sp):
         to_res(k).start()
+    mixeds.pump(2)
     for k in range(1, n_sp):
         when(back(k) < owners, lambda: from_exit(k).wait_recv())
 
@@ -568,18 +698,21 @@
             wide(out_value[:, broad]) + dot(short(key_end), exit_short, 1, 0)
         )
 
+    for step in range(3, n_sp // 2):
+        mixeds.pump(step)
+    mixeds.finish()
     for k in range(1, n_sp):
         from_res(k).wait_recv()
-    width = mixed_ref.shape[1]
+    width = mixed.shape[-1]
     step = min(width, 256)
     for c in range(0, width, step):
         total = jnp.zeros((features, step), jnp.float32)
         for s in range(n_sp):
-            total = total + dot(
-                resid_all[s], mixed_ref[s * tokens : (s + 1) * tokens, c : c + step], 0, 0
-            )
+            block = mixed_all[s, :, :, c : c + step].reshape(tokens, step)
+            total = total + dot(resid_all[s], block, 0, 0)
         out_proj[:, c : c + step] = total
 
+    mixeds.drain()
     for k in range(1, n_sp):
         to_tot(k).wait_send()
         to_res(k).wait_send()
@@ -587,51 +720,153 @@
         when(sp < owners, lambda: to_exit(k).wait_send())
 
 
-def attention_call(n_sp, n_tp, resid, proj, mixed, query, key, value, decay, state):
+def layer_kernel(n_sp, n_tp, cap, owners, names, *given):
+    refs = types.SimpleNamespace(**dict(zip(names, given, strict=True)))
+    sp, tp = lax.axis_index("sp"), lax.axis_index("tp")
+    loads = [
+        pltpu.make_async_copy(a, b, refs.more_sem.at[i])
+        for i, (a, b) in enumerate(
+            (
+                (refs.query_hbm, refs.query_ref), (refs.decay_hbm, refs.decay_ref),
+                (refs.mixed_hbm, refs.mixed), (refs.key_hbm, refs.key_ref),
+                (refs.value_hbm, refs.value_ref), (refs.state_hbm, refs.state_ref),
+            )
+        )
+    ]
+    projs = Spread(
+        n_sp, sp, tp, refs.proj, refs.proj_all, refs.pu_s, refs.pu_r, refs.pd_s, refs.pd_r,
+        refs.px_s, refs.px_r,
+    )
+    mixeds = Spread(
+        n_sp, sp, tp, refs.mixed, refs.mixed_all, refs.mu_s, refs.mu_r, refs.md_s, refs.md_r,
+        refs.mx_s, refs.mx_r,
+    )
+    drain = expert_phase(n_sp, n_tp, cap, projs, loads, refs)
+    projs.finish()
+    attention_phase(n_sp, n_tp, owners, mixeds, loads, refs)
+    projs.drain()
+    drain()
+
+
+def in_hbm(*arrays):
+    return [pltpu.with_memory_space_constraint(array, pltpu.HBM) for array in arrays]
+
+
+def store_kernel(count, *refs):
+    sems = refs[-1]
+    copies = [
+        pltpu.make_async_copy(refs[i], refs[count + i], sems.at[i]) for i in range(count)
+    ]
+    for copy in copies:
+        copy.start()
+    for copy in copies:
+        copy.wait()
+
+
+def store_call(arrays):
+    count = len(arrays)
+    return pl.pallas_call(
+        functools.partial(store_kernel, count),
+        in_specs=[pl.BlockSpec(memory_space=pltpu.VMEM)] * count,
+        out_specs=[pl.BlockSpec(memory_space=pltpu.HBM)] * count,
+        out_shape=[jax.ShapeDtypeStruct(a.shape, a.dtype) for a in arrays],
+        scratch_shapes=[pltpu.SemaphoreType.DMA((count,))],
+        compiler_params=pltpu.CompilerParams(vmem_limit_bytes=2 * 2**20),
+        name="store",
+    )(*arrays)
+
+
+def layer_call(
+    n_sp, n_tp, ids, weights, resid, cot, gain, gate, up, down, proj, mixed, query, key, value,
+    decay, state,
+):
     tokens, model = resid.shape
-    width = value.shape[1]
+    fs = gate.shape[1]
+    cap = -(-(3 * tokens // n_sp) // 16) * 16
+    cs = model // n_tp
+    rows = n_sp * cap
+    n_y = n_tp // CORES
+    pieces = n_sp if n_sp <= 8 else 1
+    features, width = proj.shape
     heads = width // DV
     channels = heads * KEY_CHANNELS
     owners = min(n_sp, channels // 16)
     share = channels // owners
-    features = model // n_sp
     bf, f32 = jnp.bfloat16, jnp.float32
-    dma = pltpu.SemaphoreType.DMA
+    vmem, dma = pltpu.VMEM, pltpu.SemaphoreType.DMA
+    side = max(1, n_y - 1)
+    many = 8 * -(-heads // 8)
+    proj = proj.reshape(2, features // 2, width)
+    mixed = mixed.reshape(2, tokens // 2, width)
+    main = pl.BlockSpec(memory_space=pltpu.HBM)
     local = pl.BlockSpec(memory_space=pltpu.VMEM)
+    inputs = {
+        "ids_hbm": ids, "weight_hbm": weights, "resid_hbm": resid, "cot_hbm": cot,
+        "gain_hbm": gain, "gate_hbm": gate, "up_hbm": up, "down_hbm": down, "proj_hbm": proj,
+        "mixed_hbm": mixed, "query_hbm": query, "key_hbm": key, "value_hbm": value,
+        "decay_hbm": decay, "state_hbm": state,
+    }
+    outputs = {
+        "ggate": (gate.shape, bf), "gup": (up.shape, bf), "gdown": (down.shape, bf),
+        "out_proj": ((features, width), f32), "out_query": (query.shape, bf),
+        "out_key": (key.shape, bf), "out_value": (value.shape, bf), "out_log": (decay.shape, f32),
+    }
+    half_line = max(1, n_sp // 2 - 1)
+    scratch = {
+        "ids_ref": vmem(ids.shape, ids.dtype), "weight_ref": vmem(weights.shape, f32),
+        "resid_ref": vmem(resid.shape, bf), "cot_ref": vmem(cot.shape, bf),
+        "gain_ref": vmem(gain.shape, f32), "proj": vmem(proj.shape, bf),
+        "gate": vmem(gate.shape, bf), "up": vmem(up.shape, bf), "down": vmem(down.shape, bf),
+        "proj_all": vmem((n_sp, *proj.shape), bf), "grad_resid": vmem(resid.shape, bf),
+        "pick": vmem((n_sp, cap, tokens), bf), "sent": vmem((n_sp, 2, cap, cs), bf),
+        "rows_in": vmem((n_tp, 2, n_sp, cap, cs), bf),
+        "gate_pre": vmem((rows, fs), f32), "up_pre": vmem((rows, fs), f32),
+        "grad_hid": vmem((rows, fs), f32), "hidden": vmem((rows, fs), bf),
+        "gact": vmem((rows, fs), bf), "uact": vmem((rows, fs), bf),
+        "pair_sent": vmem((n_y, rows, cs), bf), "pair_got": vmem((n_y, rows, cs), bf),
+        "own_sum": vmem((n_sp, cap, cs), f32), "side_sent": vmem((side, n_sp, cap, cs), bf),
+        "side_got": vmem((side, n_sp, cap, cs), bf), "final": vmem((n_sp, cap, cs), bf),
+        "back": vmem((n_sp, cap, cs), bf), "gathered": vmem((n_tp, tokens, cs), bf),
+        "mixed": vmem(mixed.shape, bf), "mixed_all": vmem((n_sp, *mixed.shape), bf),
+        "query_ref": vmem(query.shape, bf), "key_ref": vmem(key.shape, bf),
+        "value_ref": vmem(value.shape, bf), "decay_ref": vmem(decay.shape, f32),
+        "state_ref": vmem(state.shape, f32), "grad": vmem((tokens, width), bf),
+        "cum": vmem((tokens, channels), f32), "own": vmem((owners, share, DV), bf),
+        "totals": vmem((many, KEY_CHANNELS), f32), "spans": vmem((n_sp, share, DV), bf),
+        "decays": vmem((n_sp, many, KEY_CHANNELS), f32), "leave": vmem((n_sp, share, DV), bf),
+        "exits": vmem((owners, share, DV), bf), "query_grad": vmem((tokens, channels), f32),
+        "key_part": vmem((tokens, channels), f32),
+        "resid_sent": vmem((n_sp, tokens, features), bf),
+        "resid_all": vmem((n_sp, tokens, features), bf),
+        "load_sem": dma((9,)), "more_sem": dma((6,)),
+    }
+    for name in ("out", "ret", "sum", "tot", "exit", "res"):
+        scratch |= {name + "_s": dma((n_sp,)), name + "_r": dma((n_sp,))}
+    for name in ("side", "twin", "red"):
+        scratch |= {name + "_s": dma((n_y, pieces)), name + "_r": dma((n_y, pieces))}
+    for name in ("pair", "gat", "gtw"):
+        scratch |= {name + "_s": dma((n_y,)), name + "_r": dma((n_y,))}
+    for name in ("pu", "pd", "mu", "md"):
+        scratch |= {name + "_s": dma((half_line, 2)), name + "_r": dma((half_line, 2))}
+    for name in ("px", "mx"):
+        scratch |= {name + "_s": dma((n_sp - 1, 2)), name + "_r": dma((n_sp - 1, 2))}
     return pl.pallas_call(
-        functools.partial(attention_kernel, n_sp, n_tp, owners),
-        in_specs=[local] * 8,
-        out_specs=[local] * 5,
-        out_shape=[
-            jax.ShapeDtypeStruct((features, width), f32),
-            jax.ShapeDtypeStruct(query.shape, bf),
-            jax.ShapeDtypeStruct(key.shape, bf),
-            jax.ShapeDtypeStruct(value.shape, bf),
-            jax.ShapeDtypeStruct(decay.shape, f32),
-        ],
-        scratch_shapes=[
-            pltpu.VMEM((tokens, width), bf),
-            pltpu.VMEM((tokens, channels), f32),
-            pltpu.VMEM((owners, share, DV), bf),
-            pltpu.VMEM((8 * -(-heads // 8), KEY_CHANNELS), f32),
-            pltpu.VMEM((n_sp, share, DV), bf),
-            pltpu.VMEM((n_sp, 8 * -(-heads // 8), KEY_CHANNELS), f32),
-            pltpu.VMEM((n_sp, share, DV), bf),
-            pltpu.VMEM((owners, share, DV), bf),
-            pltpu.VMEM((tokens, channels), f32),
-            pltpu.VMEM((tokens, channels), f32),
-            pltpu.VMEM((n_sp, tokens, features), bf),
-            pltpu.VMEM((n_sp, tokens, features), bf),
-            *([dma((n_sp,))] * 8),
-        ],
+        functools.partial(
+            layer_kernel, n_sp, n_tp, cap, owners, [*inputs, *outputs, *scratch]
+        ),
+        in_specs=[main] * len(inputs),
+        out_specs=[local] * len(outputs),
+        out_shape=[jax.ShapeDtypeStruct(*kind) for kind in outputs.values()],
+        scratch_shapes=list(scratch.values()),
         compiler_params=pltpu.CompilerParams(
-            collective_id=1, has_side_effects=True, vmem_limit_bytes=40 * 2**20
+            collective_id=0, has_side_effects=True, vmem_limit_bytes=42 * 2**20
         ),
         cost_estimate=pl.CostEstimate(
-            flops=10**10, bytes_accessed=2 * model * width, transcendentals=8 * tokens * channels
+            flops=24 * rows * model * fs, bytes_accessed=12 * model * fs,
+            transcendentals=rows * fs,
         ),
-        name="attention",
-    )(resid, proj, mixed, query, key, value, decay, state)
+        name="layer",
+    )(*in_hbm(*inputs.values()))
 
 
 def on_device(
@@ -653,25 +888,13 @@
 ):
     n_sp = lax.axis_size("sp")
     n_tp = lax.axis_size("tp")
-    proj_all = lax.all_gather(out_proj, "sp", axis=0, tiled=True)
-    mixed_all = lax.all_gather(mixed, "sp", axis=0, tiled=True)
-    grad_resid, grad_gate, grad_up, grad_down = expert_call(
+    grads = layer_call(
         n_sp, n_tp, route_ids.T, route_weight.T, resid, cotangent, norm_gain.reshape(1, -1),
-        expert_gate[0], expert_up[0], expert_down[0],
+        expert_gate[0], expert_up[0], expert_down[0], out_proj, mixed, query, key, value,
+        log_decay, span_state[0],
     )
-    grad_proj, grad_query, grad_key, grad_value, grad_log = attention_call(
-        n_sp, n_tp, grad_resid, proj_all, mixed_all, query, key, value, log_decay, span_state[0]
-    )
-    return (
-        grad_gate[None],
-        grad_up[None],
-        grad_down[None],
-        grad_proj,
-        grad_query,
-        grad_key,
-        grad_value,
-        grad_log,
-    )
+    stored = store_call(grads)
+    return (*(grad[None] for grad in stored[:3]), *stored[3:])
 
 
 def solution(mesh):

time: 200 us -> 119 us (0.59)
  waiting for transfers between devices: 75.8 us -> 0 us
  Pallas kernels: 91.4 us -> 118 us
  local copies, waits for them, and re-layouts: 17.6 us -> 0 us
  between operations: 14.1 us -> 0.65 us
    all_gather x2 -> x0, waiting for transfers between devices: 74.4 us -> none  [the longest x1 73.8 us: on_device(): proj_all = lax.all_gather(out_proj, 'sp', axis=0, tiled=True)]
    pallas_call x2, Pallas kernels: 91.4 us -> 118 us  [the longest x1 115 us: layer_call(): pl.pallas_call(functools.partial(layer_kernel, n_sp, n_tp, cap, owners, [...]
    unnamed x38 -> x0, local copies, waits for them, and re-layouts: 17.6 us -> none
  transfers between devices with their start and end apart: 2 -> 0, of which waited for: 2 -> 0; matrix products, arithmetic and copies ran while one was open for 0% -> 0% of each run, Pallas kernels for 33% -> 0%
where the time goes in v2:
time: 119 us
  Pallas kernels  118 us (99%)
    pallas_call x1, Pallas kernels, layer_call(): pl.pallas_call(functools.partial(layer_kernel, n_sp, n_tp, cap, owners, [...  115 us
    pallas_call x1, Pallas kernels, store_call(): pl.pallas_call(functools.partial(store_kernel, count), in_specs=[pl.Block...  3.26 us

profile of v2, /device:TPU:0, one launch (start us, length us, event | category | flops | bytes accessed | tf_op | source)
XLA Modules:
  0.0 119.1 jit_solution(1886690077899340526)
XLA Ops:
  0.6 115.2 %layer.1 = (bf16[2048,512]{1,0:T(8,128)(2,1)S(1)}, bf16[2048,512]{1,0:T(8,128)(2,1)S(1)}, bf16[512,2048]{1,0:T(8,128)(2,1)S(1)}, f32[256,1024]{1,0:T(8,128)S(1)}...) custom-call(s32[2,128]{1,0:T(2,128)} %bitcast.22, ...), custom_call_target="tpu_custom_call" | custom-call | flops 9663676416 | bytes 12582912 | tf_op jit(solution)/shard_map/layer/pallas_call | solution.py:853
  115.8 3.3 %store.1 = (bf16[2048,512]{1,0:T(8,128)(2,1)}, bf16[2048,512]{1,0:T(8,128)(2,1)}, bf16[512,2048]{1,0:T(8,128)(2,1)}, f32[256,1024]{1,0:T(8,128)}, bf16[128,512]{...) custom-call(bf16[2048,512]{1,0:T(8,128)(2,1)S(1)} %get-tuple-element.24.refs_0_, ...), custom_call_target="tpu_custom_call" | custom-call | tf_op jit(solution)/shard_map/store/pallas_call | solution.py:768

commit v3 on v2

--- a/solution.py
+++ b/solution.py
@@ -43,6 +43,15 @@
         src_ref=src, dst_ref=dst, send_sem=send, recv_sem=recv, device_id=device,
         device_id_type=MESH,
     )
+
+
+def peer(sp, k):
+    place = 1
+    while place <= k:
+        if k // place % 2:
+            sp = sp + place * (1 - 2 * lax.rem(lax.div(sp, place), 2))
+        place *= 2
+    return sp
 
 
 def greet(sp, tp, n_sp, n_tp):
@@ -143,7 +152,7 @@
                     )
 
 
-def expert_phase(n_sp, n_tp, cap, projs, later, refs):
+def expert_phase(n_sp, n_tp, cap, projs, mixeds, later, refs):
     ids_hbm = refs.ids_hbm
     weight_hbm = refs.weight_hbm
     resid_hbm = refs.resid_hbm
@@ -264,14 +273,16 @@
 
     for load in later:
         load.start()
+    for load in later:
+        load.wait()
     pl.semaphore_wait(barrier, others)
 
     def outgoing(k):
-        d = lax.rem(sp + k, n_sp)
+        d = peer(sp, k)
         return remote(sent.at[d], rows_in.at[tp, :, sp], out_s.at[k], out_r.at[k], (d, tp))
 
     def incoming(k):
-        s = lax.rem(sp - k + n_sp, n_sp)
+        s = peer(sp, k)
         return remote(sent.at[s], rows_in.at[tp, :, s], out_s.at[k], out_r.at[k], (s, tp))
 
     for k in range(1, n_sp):
@@ -286,7 +297,7 @@
     def piece(t, k):
         if not chunked:
             return rows_in.at[t]
-        return rows_in.at[t, :, lax.rem(sp - k + n_sp, n_sp)]
+        return rows_in.at[t, :, peer(sp, k)]
 
     def to_side(j, k):
         return remote(
@@ -323,7 +334,6 @@
     for k in range(pieces):
         for j in range(n_y):
             from_twin(j, k).wait_recv()
-    projs.pump(1)
 
     gate_pre[...] = jnp.zeros_like(gate_pre)
     up_pre[...] = jnp.zeros_like(up_pre)
@@ -337,6 +347,7 @@
         up_pre[...] += dot(block, up[part, :], 1, 0)
         grad_hid[...] += dot(rows_in[p, 1].reshape(rows, cs), down[:, part], 1, 1)
 
+    projs.pump(1)
     @pl.loop(0, n_sp)
     def _(s):
         part = pl.ds(pl.multiple_of(s * cap, 16), cap)
@@ -359,7 +370,7 @@
         to_pair(i).start()
 
     def span(k):
-        return lax.rem(sp + k, n_sp)
+        return peer(sp, k)
 
     def to_red(j, k):
         dev = (sp, at_y(j))
@@ -372,7 +383,7 @@
             red_s.at[j, k], red_r.at[j, k], dev,
         )
 
-    order = list(range(1, n_sp)) + [0]
+    order = list(range(n_sp - 1, -1, -1))
     for j in range(n_y):
         i = (j + 1) % n_y
         value = partial(at_y(i))
@@ -408,7 +419,7 @@
         return remote(final.at[span(k)], back.at[sp], ret_s.at[k], ret_r.at[k], (span(k), tp))
 
     def from_back(k):
-        s = lax.rem(sp - k + n_sp, n_sp)
+        s = peer(sp, k)
         return remote(final.at[s], back.at[s], ret_s.at[k], ret_r.at[k], (s, tp))
 
     fill(n_tp // 2)
@@ -476,6 +487,7 @@
 
     for step in range(3, n_sp // 2):
         projs.pump(step)
+    mixeds.start()
 
     def drain():
         for k in range(1, n_sp):
@@ -496,7 +508,88 @@
     return drain
 
 
-def attention_phase(n_sp, n_tp, owners, mixeds, loads, refs):
+class Slices:
+    def __init__(self, n_sp, n_tp, sp, tp, refs):
+        self.n_sp, self.n_tp, self.sp, self.tp, self.refs = n_sp, n_tp, sp, tp, refs
+        self.core, self.y = lax.rem(tp, CORES), lax.div(tp, CORES)
+
+    def bearer(self, k):
+        return lax.rem(peer(self.sp, k) + self.sp, self.n_tp)
+
+    def holds(self, k):
+        return self.tp == self.bearer(k)
+
+    def same(self, k):
+        return lax.rem(self.bearer(k), CORES) == self.core
+
+    def over(self, k):
+        refs, d = self.refs, peer(self.sp, k)
+        return remote(
+            refs.resid_sent.at[d], refs.resid_all.at[self.sp], refs.res_s.at[k],
+            refs.res_r.at[k], (d, self.tp),
+        )
+
+    def got(self, k):
+        refs, d = self.refs, peer(self.sp, k)
+        there = refs.resid_all.at[d]
+        return remote(there, there, refs.res_s.at[k], refs.res_r.at[k], (d, self.tp))
+
+    def side(self, k, j):
+        refs = self.refs
+        there = refs.resid_all.at[peer(self.sp, k)]
+        t = CORES * lax.rem(self.y + j, self.n_tp // CORES) + self.core
+        return remote(there, there, refs.rsi_s.at[j, k], refs.rsi_r.at[k], (self.sp, t))
+
+    def twin(self, k):
+        refs = self.refs
+        there = refs.resid_all.at[peer(self.sp, k)]
+        t = CORES * self.y + 1 - self.core
+        return remote(there, there, refs.rtw_s.at[k], refs.rtw_r.at[k], (self.sp, t))
+
+    def sides(self):
+        return range(1, self.n_tp // CORES)
+
+    def send(self):
+        refs = self.refs
+        features = refs.grad_resid.shape[1] // self.n_sp
+        for d in range(self.n_sp):
+            refs.resid_sent[d] = refs.grad_resid[:, d * features : (d + 1) * features]
+        for k in range(self.n_sp - 1, 0, -1):
+            pl.when(self.holds(k))(lambda: self.over(k).start())
+        refs.resid_all[self.sp] = refs.resid_sent[self.sp]
+
+    def spread(self):
+        for k in range(1, self.n_sp):
+            @pl.when(self.holds(k))
+            def _():
+                self.got(k).wait_recv()
+                for j in self.sides():
+                    self.side(k, j).start()
+                self.twin(k).start()
+
+    def relay(self):
+        for k in range(1, self.n_sp):
+            @pl.when(jnp.logical_and(self.same(k), jnp.logical_not(self.holds(k))))
+            def _():
+                self.side(k, 1).wait_recv()
+                self.twin(k).start()
+
+    def finish(self):
+        for k in range(1, self.n_sp):
+            pl.when(jnp.logical_not(self.same(k)))(lambda: self.twin(k).wait_recv())
+
+    def drain(self):
+        for k in range(1, self.n_sp):
+            @pl.when(self.holds(k))
+            def _():
+                self.over(k).wait_send()
+                for j in self.sides():
+                    self.side(k, j).wait_send()
+
+            pl.when(self.same(k))(lambda: self.twin(k).wait_send())
+
+
+def attention_phase(n_sp, n_tp, owners, mixeds, slices, refs):
     query_hbm = refs.query_hbm
     key_hbm = refs.key_hbm
     value_hbm = refs.value_hbm
@@ -547,12 +640,7 @@
     lower = triangle(tokens, False)
     ones = lower.astype(jnp.float32)
 
-    for d in range(n_sp):
-        resid_sent[d] = grad_resid[:, d * features : (d + 1) * features]
     totals[...] = jnp.zeros_like(totals)
-    for load in loads:
-        load.wait()
-    mixeds.start()
     mixed_all[sp] = mixed[...]
     for h in range(heads):
         narrow = slice(h * KEY_CHANNELS, (h + 1) * KEY_CHANNELS)
@@ -572,10 +660,9 @@
         totals[h : h + 1, :] = jnp.exp(cum_h[tokens - 1 : tokens, :])
 
     def there(k):
-        return lax.rem(sp + k, n_sp)
-
-    def back(k):
-        return lax.rem(sp - k + n_sp, n_sp)
+        return peer(sp, k)
+
+    back = there
 
     def when(test, action):
         if owners == n_sp:
@@ -601,21 +688,10 @@
     def from_exit(k):
         return remote(exits.at[back(k)], exits.at[back(k)], exit_s.at[k], exit_r.at[k], (back(k), tp))
 
-    def to_res(k):
-        return remote(
-            resid_sent.at[there(k)], resid_all.at[sp], res_s.at[k], res_r.at[k], (there(k), tp)
-        )
-
-    def from_res(k):
-        return remote(
-            resid_all.at[back(k)], resid_all.at[back(k)], res_s.at[k], res_r.at[k], (back(k), tp)
-        )
-
-    for k in range(1, n_sp):
+    for k in range(n_sp - 1, 0, -1):
         to_tot(k).start()
         when(there(k) < owners, lambda: to_sum(k).start())
     decays[sp] = totals[...]
-    resid_all[sp] = resid_sent[sp]
 
     @functools.partial(when, sp < owners)
     def _():
@@ -665,11 +741,11 @@
                 running = wide(spans[s]) + factor * running
         exits[sp] = leave[sp]
 
-    for k in range(1, n_sp):
+    for k in range(n_sp - 1, 0, -1):
         when(sp < owners, lambda: to_exit(k).start())
-    for k in range(1, n_sp):
-        to_res(k).start()
+    slices.spread()
     mixeds.pump(2)
+    slices.relay()
     for k in range(1, n_sp):
         when(back(k) < owners, lambda: from_exit(k).wait_recv())
 
@@ -701,8 +777,7 @@
     for step in range(3, n_sp // 2):
         mixeds.pump(step)
     mixeds.finish()
-    for k in range(1, n_sp):
-        from_res(k).wait_recv()
+    slices.finish()
     width = mixed.shape[-1]
     step = min(width, 256)
     for c in range(0, width, step):
@@ -713,9 +788,9 @@
         out_proj[:, c : c + step] = total
 
     mixeds.drain()
+    slices.drain()
     for k in range(1, n_sp):
         to_tot(k).wait_send()
-        to_res(k).wait_send()
         when(there(k) < owners, lambda: to_sum(k).wait_send())
         when(sp < owners, lambda: to_exit(k).wait_send())
 
@@ -741,9 +816,11 @@
         n_sp, sp, tp, refs.mixed, refs.mixed_all, refs.mu_s, refs.mu_r, refs.md_s, refs.md_r,
         refs.mx_s, refs.mx_r,
     )
-    drain = expert_phase(n_sp, n_tp, cap, projs, loads, refs)
+    slices = Slices(n_sp, n_tp, sp, tp, refs)
+    drain = expert_phase(n_sp, n_tp, cap, projs, mixeds, loads, refs)
+    slices.send()
     projs.finish()
-    attention_phase(n_sp, n_tp, owners, mixeds, loads, refs)
+    attention_phase(n_sp, n_tp, owners, mixeds, slices, refs)
     projs.drain()
     drain()
 
@@ -848,6 +925,10 @@
         scratch |= {name + "_s": dma((n_y,)), name + "_r": dma((n_y,))}
     for name in ("pu", "pd", "mu", "md"):
         scratch |= {name + "_s": dma((half_line, 2)), name + "_r": dma((half_line, 2))}
+    scratch |= {
+        "rsi_s": dma((n_y, n_sp)), "rsi_r": dma((n_sp,)), "rtw_s": dma((n_sp,)),
+        "rtw_r": dma((n_sp,)),
+    }
     for name in ("px", "mx"):
         scratch |= {name + "_s": dma((n_sp - 1, 2)), name + "_r": dma((n_sp - 1, 2))}
     return pl.pallas_call(

time: 119 us -> 115 us (0.966)
  Pallas kernels: 118 us -> 114 us
    pallas_call x1, Pallas kernels: 115 us -> 111 us  [layer_call(): pl.pallas_call(functools.partial(layer_kernel, n_sp, n_tp, cap, owners, [...]
where the time goes in v3:
time: 115 us
  Pallas kernels  114 us (99%)
    pallas_call x1, Pallas kernels, layer_call(): pl.pallas_call(functools.partial(layer_kernel, n_sp, n_tp, cap, owners, [...  111 us
    pallas_call x1, Pallas kernels, store_call(): pl.pallas_call(functools.partial(store_kernel, count), in_specs=[pl.Block...  3.26 us

profile of v3, /device:TPU:0, one launch (start us, length us, event | category | flops | bytes accessed | tf_op | source)
XLA Modules:
  0.0 114.7 jit_solution(10408248095046380921)
XLA Ops:
  0.6 110.8 %layer.1 = (bf16[2048,512]{1,0:T(8,128)(2,1)S(1)}, bf16[2048,512]{1,0:T(8,128)(2,1)S(1)}, bf16[512,2048]{1,0:T(8,128)(2,1)S(1)}, f32[256,1024]{1,0:T(8,128)S(1)}...) custom-call(s32[2,128]{1,0:T(2,128)} %bitcast.22, ...), custom_call_target="tpu_custom_call" | custom-call | flops 9663676416 | bytes 12582912 | tf_op jit(solution)/shard_map/layer/pallas_call | solution.py:934
  111.5 3.3 %store.1 = (bf16[2048,512]{1,0:T(8,128)(2,1)}, bf16[2048,512]{1,0:T(8,128)(2,1)}, bf16[512,2048]{1,0:T(8,128)(2,1)}, f32[256,1024]{1,0:T(8,128)}, bf16[128,512]{...) custom-call(bf16[2048,512]{1,0:T(8,128)(2,1)S(1)} %get-tuple-element.24.refs_0_, ...), custom_call_target="tpu_custom_call" | custom-call | tf_op jit(solution)/shard_map/store/pallas_call | solution.py:845

commit v4 on v3

--- a/solution.py
+++ b/solution.py
@@ -130,8 +130,8 @@
                         )
                     self.across(way, step, half).start()
 
-    def finish(self):
-        for half in range(2):
+    def finish(self, halves=(0, 1)):
+        for half in halves:
             self.across(1, 0, half, True).wait_recv()
             for step in range(1, self.count):
                 for way in (1, -1):
@@ -226,7 +226,9 @@
         for i, (a, b) in enumerate(
             (
                 (resid_hbm, resid_ref), (cot_hbm, cot_ref), (ids_hbm, ids_ref),
-                (weight_hbm, weight_ref), (gain_hbm, gain_ref), (proj_hbm, proj),
+                (weight_hbm, weight_ref), (gain_hbm, gain_ref),
+                (proj_hbm.at[:, 0 : proj.shape[2]], proj.at[0]),
+                (proj_hbm.at[:, proj.shape[2] : 2 * proj.shape[2]], proj.at[1]),
                 (gate_hbm, gate), (up_hbm, up), (down_hbm, down),
             )
         )
@@ -287,7 +289,8 @@
 
     for k in range(1, n_sp):
         outgoing(k).start()
-    loads[5].wait()
+    for load in loads[5:7]:
+        load.wait()
     projs.start()
     proj_all[sp] = proj[...]
     rows_in[tp, :, sp] = sent[sp]
@@ -329,7 +332,7 @@
         for j in range(1, n_y):
             from_side(j, k).wait_recv()
             to_twin(j, k).start()
-    for load in loads[6:]:
+    for load in loads[7:]:
         load.wait()
     for k in range(pieces):
         for j in range(n_y):
@@ -439,6 +442,7 @@
     fill(units)
     projs.pump(2)
 
+    decay_phase(refs)
     for k in range(1, n_sp):
         from_back(k).wait_recv()
     gathered[tp] = short(
@@ -487,7 +491,6 @@
 
     for step in range(3, n_sp // 2):
         projs.pump(step)
-    mixeds.start()
 
     def drain():
         for k in range(1, n_sp):
@@ -589,7 +592,18 @@
             pl.when(self.same(k))(lambda: self.twin(k).wait_send())
 
 
-def attention_phase(n_sp, n_tp, owners, mixeds, slices, refs):
+def decay_phase(refs):
+    tokens = refs.cum.shape[0]
+    ones = triangle(tokens, False).astype(jnp.float32)
+    refs.totals[...] = jnp.zeros_like(refs.totals)
+    for h in range(refs.cum.shape[1] // KEY_CHANNELS):
+        narrow = slice(h * KEY_CHANNELS, (h + 1) * KEY_CHANNELS)
+        cum = dot(ones, refs.decay_ref[:, narrow], 1, 0, highest)
+        refs.cum[:, narrow] = cum
+        refs.totals[h : h + 1, :] = jnp.exp(cum[tokens - 1 : tokens, :])
+
+
+def attention_phase(n_sp, n_tp, owners, projs, mixeds, slices, refs):
     query_hbm = refs.query_hbm
     key_hbm = refs.key_hbm
     value_hbm = refs.value_hbm
@@ -640,25 +654,6 @@
     lower = triangle(tokens, False)
     ones = lower.astype(jnp.float32)
 
-    totals[...] = jnp.zeros_like(totals)
-    mixed_all[sp] = mixed[...]
-    for h in range(heads):
-        narrow = slice(h * KEY_CHANNELS, (h + 1) * KEY_CHANNELS)
-        broad = slice(h * DV, (h + 1) * DV)
-        proj_h = proj_all[:, :, :, broad].reshape(grad_resid.shape[1], DV)
-        grad_h = short(dot(grad_resid[...], proj_h, 1, 0))
-        grad[:, broad] = grad_h
-        cum_h = dot(ones, decay_ref[:, narrow], 1, 0, highest)
-        cum[:, narrow] = cum_h
-        query = wide(query_ref[:, narrow]) * scale
-        mine = short(dot(short(query * jnp.exp(cum_h)), grad_h, 0, 0))
-        if share >= KEY_CHANNELS:
-            own[h * KEY_CHANNELS // share, 0:KEY_CHANNELS] = mine
-        else:
-            each = KEY_CHANNELS // share
-            own[h * each : (h + 1) * each] = mine.reshape(each, share, DV)
-        totals[h : h + 1, :] = jnp.exp(cum_h[tokens - 1 : tokens, :])
-
     def there(k):
         return peer(sp, k)
 
@@ -688,10 +683,43 @@
     def from_exit(k):
         return remote(exits.at[back(k)], exits.at[back(k)], exit_s.at[k], exit_r.at[k], (back(k), tp))
 
+    mixed_all[sp] = mixed[...]
     for k in range(n_sp - 1, 0, -1):
         to_tot(k).start()
-        when(there(k) < owners, lambda: to_sum(k).start())
     decays[sp] = totals[...]
+    groups = 2 if heads % 2 == 0 else 1
+    per = heads // groups
+    for g in range(groups):
+        projs.finish((g,) if groups == 2 else (0, 1))
+        for h in range(g * per, (g + 1) * per):
+            narrow = slice(h * KEY_CHANNELS, (h + 1) * KEY_CHANNELS)
+            broad = slice(h * DV, (h + 1) * DV)
+            if groups == 2:
+                start = (h - g * per) * DV
+                block = proj_all[:, g, :, start : start + DV]
+                grad_h = short(dot(grad_resid[...], block.reshape(-1, DV), 1, 0))
+            else:
+                wide_half = proj_all.shape[3]
+                grad_h = jnp.concatenate(
+                    [
+                        dot(grad_resid[...], proj_all[:, i].reshape(-1, wide_half), 1, 0)
+                        for i in range(2)
+                    ],
+                    axis=1,
+                )
+                grad_h = short(grad_h[:, broad])
+            grad[:, broad] = grad_h
+            query = wide(query_ref[:, narrow]) * scale
+            mine = short(dot(short(query * jnp.exp(cum[:, narrow])), grad_h, 0, 0))
+            each = KEY_CHANNELS // share
+            own[h * each : (h + 1) * each] = mine.reshape(each, share, DV)
+        if g == 0:
+            mixeds.start()
+        least, most = owners * g // groups, owners * (g + 1) // groups
+        for k in range(n_sp - 1, 0, -1):
+            pl.when(jnp.logical_and(there(k) >= least, there(k) < most))(
+                lambda: to_sum(k).start()
+            )
 
     @functools.partial(when, sp < owners)
     def _():
@@ -819,8 +847,7 @@
     slices = Slices(n_sp, n_tp, sp, tp, refs)
     drain = expert_phase(n_sp, n_tp, cap, projs, mixeds, loads, refs)
     slices.send()
-    projs.finish()
-    attention_phase(n_sp, n_tp, owners, mixeds, slices, refs)
+    attention_phase(n_sp, n_tp, owners, projs, mixeds, slices, refs)
     projs.drain()
     drain()
 
@@ -873,7 +900,6 @@
     vmem, dma = pltpu.VMEM, pltpu.SemaphoreType.DMA
     side = max(1, n_y - 1)
     many = 8 * -(-heads // 8)
-    proj = proj.reshape(2, features // 2, width)
     mixed = mixed.reshape(2, tokens // 2, width)
     main = pl.BlockSpec(memory_space=pltpu.HBM)
     local = pl.BlockSpec(memory_space=pltpu.VMEM)
@@ -892,9 +918,9 @@
     scratch = {
         "ids_ref": vmem(ids.shape, ids.dtype), "weight_ref": vmem(weights.shape, f32),
         "resid_ref": vmem(resid.shape, bf), "cot_ref": vmem(cot.shape, bf),
-        "gain_ref": vmem(gain.shape, f32), "proj": vmem(proj.shape, bf),
+        "gain_ref": vmem(gain.shape, f32), "proj": vmem((2, features, width // 2), bf),
         "gate": vmem(gate.shape, bf), "up": vmem(up.shape, bf), "down": vmem(down.shape, bf),
-        "proj_all": vmem((n_sp, *proj.shape), bf), "grad_resid": vmem(resid.shape, bf),
+        "proj_all": vmem((n_sp, 2, features, width // 2), bf), "grad_resid": vmem(resid.shape, bf),
         "pick": vmem((n_sp, cap, tokens), bf), "sent": vmem((n_sp, 2, cap, cs), bf),
         "rows_in": vmem((n_tp, 2, n_sp, cap, cs), bf),
         "gate_pre": vmem((rows, fs), f32), "up_pre": vmem((rows, fs), f32),
@@ -915,7 +941,7 @@
         "key_part": vmem((tokens, channels), f32),
         "resid_sent": vmem((n_sp, tokens, features), bf),
         "resid_all": vmem((n_sp, tokens, features), bf),
-        "load_sem": dma((9,)), "more_sem": dma((6,)),
+        "load_sem": dma((10,)), "more_sem": dma((6,)),
     }
     for name in ("out", "ret", "sum", "tot", "exit", "res"):
         scratch |= {name + "_s": dma((n_sp,)), name + "_r": dma((n_sp,))}

time: 115 us -> 114 us (level)
  no operation moved by 1% of the time
where the time goes in v4:
time: 114 us
  Pallas kernels  113 us (99%)
    pallas_call x1, Pallas kernels, layer_call(): pl.pallas_call(functools.partial(layer_kernel, n_sp, n_tp, cap, owners, [...  110 us
    pallas_call x1, Pallas kernels, store_call(): pl.pallas_call(functools.partial(store_kernel, count), in_specs=[pl.Block...  3.26 us

profile of v4, /device:TPU:0, one launch (start us, length us, event | category | flops | bytes accessed | tf_op | source)
XLA Modules:
  0.0 113.7 jit_solution(17955500697403008518)
XLA Ops:
  0.6 109.8 %layer.1 = (bf16[2048,512]{1,0:T(8,128)(2,1)S(1)}, bf16[2048,512]{1,0:T(8,128)(2,1)S(1)}, bf16[512,2048]{1,0:T(8,128)(2,1)S(1)}, f32[256,1024]{1,0:T(8,128)S(1)}...) custom-call(s32[2,128]{1,0:T(2,128)} %bitcast.20, ...), custom_call_target="tpu_custom_call" | custom-call | flops 9663676416 | bytes 12582912 | tf_op jit(solution)/shard_map/layer/pallas_call | solution.py:960
  110.4 3.3 %store.1 = (bf16[2048,512]{1,0:T(8,128)(2,1)}, bf16[2048,512]{1,0:T(8,128)(2,1)}, bf16[512,2048]{1,0:T(8,128)(2,1)}, f32[256,1024]{1,0:T(8,128)}, bf16[128,512]{...) custom-call(bf16[2048,512]{1,0:T(8,128)(2,1)S(1)} %get-tuple-element.24.refs_0_, ...), custom_call_target="tpu_custom_call" | custom-call | tf_op jit(solution)/shard_map/store/pallas_call | solution.py:872
